TPU v7x, 256 devices: a whole 4x4x8 slice. The times are simulated.
256 devices in a mesh: rep: 2 (over z_hi), fs: 16 (over z_lo, y), tp: 8 (over x, core).
Axes of the slice: x: 4, y: 4, z: 8 (z_hi: 2, z_lo: 4; z = z_hi * 4 + z_lo), core: 2. Of those that a mesh axis runs over, the one named last changes fastest.
Arguments:
- stream: bfloat16 [16384, 2048], P(('rep', 'fs'), 'tp'), may hold values from -6 to 6
- recurrent_norm_gain: float32 [2048], replicated, may hold values from 0.1 to 1.9
- feedforward_norm_gain: float32 [2048], replicated, may hold values from 0.1 to 1.9
- recurrent_input_weight: bfloat16 [2048, 2048], P('fs', 'tp'), may hold values from -0.125 to 0.125
- output_gate_weight: bfloat16 [2048, 2048], P('fs', 'tp'), may hold values from -0.125 to 0.125
- causal_filter_weight: bfloat16 [4, 2048], P(None, 'tp'), may hold values from -3 to 3
- decay_gate_matrix: bfloat16 [32, 64, 64], P('tp'), may hold values from -0.75 to 0.75
- input_gate_matrix: bfloat16 [32, 64, 64], P('tp'), may hold values from -0.75 to 0.75
- channel_decay_param: float32 [2048], P('tp'), may hold values from 3 to 10
- token_decay_offset: float32 [16384, 2048], P(('rep', 'fs'), 'tp'), may hold values from -0.7 to 0, as said below
- recurrent_output_weight: bfloat16 [2048, 2048], P('tp', 'fs'), may hold values from -0.125 to 0.125
- up_projection_weight: bfloat16 [2048, 6144], P('fs', 'tp'), may hold values from -0.125 to 0.125
- down_projection_weight: bfloat16 [6144, 2048], P('tp', 'fs'), may hold values from -0.078125 to 0.078125
Outputs:
- updated: bfloat16 [16384, 2048], P(('rep', 'fs'), 'tp')
Inputs may be any that keep to these rules, and one draw needn't show every extreme that they name: `token_decay_offset`: zero except at a few positions, where a whole row is negative.
All inputs are finite; a program needn't handle non-finite values.
Results may differ from a plain program's by a relative error of at most 0.015.
Values may be sent and summed in bfloat16 or wider, within the bound.
A program may use at most 64 MiB of HBM per device.

v0:
```python
import jax
import jax.numpy as jnp
from jax import lax
from jax.sharding import Mesh
from jax.sharding import PartitionSpec as P

SEQ_LEN = 128
FS = ("fs_0", "fs_1")
REP_FS = ("rep", "fs_0", "fs_1")


EPSILON = 1e-06
DECAY_MULTIPLIER = 8.0


def in_order(pieces, dim):
    shape = list(pieces.shape[1:])
    shape[dim] *= pieces.shape[0]
    return jnp.moveaxis(pieces, 0, dim).reshape(shape)


def from_everyone(value, axis):
    copies = jnp.broadcast_to(value, (lax.axis_size(axis), *value.shape))
    return lax.all_to_all(copies, axis, split_axis=0, concat_axis=0, tiled=True)


def gather_directly(value, axis, dim):
    return in_order(from_everyone(value, axis), dim)


def in_one_piece(arrays, axis, dim, along):
    ends, at = ([], 0)
    for a in arrays[:-1]:
        at += a.shape[along]
        ends.append(at)
    both = jnp.concatenate(arrays, axis=along)
    return tuple(jnp.split(lax.all_gather(both, axis, axis=dim, tiled=True), ends, axis=along))


def split_up(value, dim, devices):
    before, after = (value.shape[:dim], value.shape[dim + 1 :])
    return jnp.moveaxis(value.reshape(*before, devices, -1, *after), dim, 0)


def sent_and_summed(value, axis, dim):
    pieces = split_up(value, dim, lax.axis_size(axis))
    arrived = lax.all_to_all(pieces, axis, split_axis=0, concat_axis=0, tiled=True)
    return arrived.astype(jnp.float32).sum(axis=0)


def gather_in_order(value, axes, order):
    pieces = value[None]
    for k in order:
        pieces = lax.all_gather(pieces, axes[k], axis=0, tiled=True)
    held = [lax.axis_size(axes[k]) for k in reversed(order)]
    pieces = pieces.reshape(*held, *value.shape)
    turned = sorted(range(len(order)), key=lambda place: order[len(order) - 1 - place])
    return pieces.transpose(*turned, *range(len(order), pieces.ndim)).reshape(-1, *value.shape)


def gather_axes(value, axes, order, dim):
    return in_order(gather_in_order(value, axes, order), dim)


def norm_rows(values, gain):
    widened = values.astype(jnp.float32)
    inverse = lax.rsqrt(jnp.mean(widened * widened, axis=-1, keepdims=True) + EPSILON)
    return (widened * inverse * gain).astype(jnp.bfloat16)


def short_filter(values, causal_filter_weight, sequence_length):
    positions, channels = values.shape
    sequences = positions // sequence_length
    reach = causal_filter_weight.shape[0]
    widened = (
        lax.optimization_barrier(values)
        .astype(jnp.float32)
        .reshape(sequences, sequence_length, channels)
    )
    padded = jnp.pad(widened, ((0, 0), (reach - 1, 0), (0, 0)))
    taps = causal_filter_weight.astype(jnp.float32)
    total = taps[0] * padded[:, 0:sequence_length]
    for offset in range(1, reach):
        total = total + taps[offset] * padded[:, offset : offset + sequence_length]
    return total.reshape(positions, channels).astype(jnp.bfloat16)


def combine(earlier, later):
    return (earlier[0] * later[0], later[0] * earlier[1] + later[1])


def recurrent_states(
    filtered_input,
    output_gate_rows,
    decay_gate_matrix,
    input_gate_matrix,
    channel_decay_param,
    token_decay_offset,
    sequence_length,
):
    positions, channels = filtered_input.shape
    blocks, block_size, _ = decay_gate_matrix.shape
    grouped = filtered_input.reshape(positions, blocks, block_size)
    recurrent_step = jax.nn.sigmoid(
        jnp.einsum(
            "tnc,ncd->tnd", grouped, decay_gate_matrix, preferred_element_type=jnp.float32
        ).reshape(positions, channels)
    )
    inputs = jax.nn.sigmoid(
        jnp.einsum(
            "tnc,ncd->tnd", grouped, input_gate_matrix, preferred_element_type=jnp.float32
        ).reshape(positions, channels)
    )
    decay_logarithm = (
        -DECAY_MULTIPLIER * recurrent_step * jax.nn.softplus(-channel_decay_param)
        + token_decay_offset
    )
    widened = lax.optimization_barrier(filtered_input).astype(jnp.float32)
    drive = jnp.sqrt(-jnp.expm1(2.0 * decay_logarithm)) * inputs * widened
    shaped = (positions // sequence_length, sequence_length, channels)
    _, states = lax.associative_scan(
        combine, (jnp.exp(decay_logarithm).reshape(shaped), drive.reshape(shaped)), axis=1
    )
    gate_wide = lax.optimization_barrier(output_gate_rows).astype(jnp.float32)
    return (states.reshape(positions, channels) * jax.nn.gelu(gate_wide, approximate=False)).astype(
        jnp.bfloat16
    )


def shards(
    stream,
    recurrent_norm_gain,
    feedforward_norm_gain,
    recurrent_input_weight,
    output_gate_weight,
    causal_filter_weight,
    decay_gate_matrix,
    input_gate_matrix,
    channel_decay_param,
    token_decay_offset,
    recurrent_output_weight,
    up_projection_weight,
    down_projection_weight,
):
    whole = gather_directly(stream, "tp", 1)
    normed = norm_rows(whole, recurrent_norm_gain)
    pieces = in_one_piece((recurrent_input_weight, output_gate_weight), FS, 0, 1)
    columns = normed
    value_total = jnp.dot(columns, pieces[0], preferred_element_type=jnp.float32)
    gate_total = jnp.dot(columns, pieces[1], preferred_element_type=jnp.float32)
    filtered_input = short_filter(value_total.astype(jnp.bfloat16), causal_filter_weight, SEQ_LEN)
    mixed_rows = recurrent_states(
        filtered_input,
        gate_total.astype(jnp.bfloat16),
        decay_gate_matrix,
        input_gate_matrix,
        channel_decay_param,
        token_decay_offset,
        SEQ_LEN,
    )
    mixer_terms = jnp.dot(
        mixed_rows,
        gather_directly(recurrent_output_weight, FS, 1),
        preferred_element_type=jnp.float32,
    )
    summed = sent_and_summed(mixer_terms.astype(jnp.bfloat16), "tp", 1)
    middle = (stream.astype(jnp.float32) + summed).astype(jnp.bfloat16)
    whole_mid = gather_directly(middle, "tp", 1)
    normed_mid = norm_rows(whole_mid, feedforward_norm_gain)
    columns = normed_mid
    raised = jnp.dot(
        columns,
        gather_axes(up_projection_weight, FS, (0, 1), 0),
        preferred_element_type=jnp.float32,
    )
    activity = jnp.square(jax.nn.relu(raised)).astype(jnp.bfloat16)
    channel_terms = jnp.dot(
        activity,
        gather_axes(down_projection_weight, FS, (0, 1), 1),
        preferred_element_type=jnp.float32,
    )
    channel_sum = sent_and_summed(channel_terms.astype(jnp.bfloat16), "tp", 1)
    return (middle.astype(jnp.float32) + channel_sum).astype(jnp.bfloat16)


def solution(mesh):
    split = Mesh(
        mesh.devices.reshape(mesh.shape["rep"], 4, 4, mesh.shape["tp"]),
        ("rep", "fs_0", "fs_1", "tp"),
    )
    placed = (
        P(REP_FS, "tp"),
        P(),
        P(),
        P(FS, "tp"),
        P(FS, "tp"),
        P(None, "tp"),
        P("tp", None, None),
        P("tp", None, None),
        P("tp"),
        P(REP_FS, "tp"),
        P("tp", FS),
        P(FS, "tp"),
        P("tp", FS),
    )
    return jax.shard_map(
        shards, mesh=split, in_specs=placed, out_specs=P(REP_FS, "tp"), check_vma=False
    )
```

profile of v0, /device:TPU:4, one launch (start us, length us, event | category | flops | bytes accessed | tf_op | source)
XLA Modules:
  0.0 235.9 jit_solution(2918589249318210032)
XLA Ops:
  6.5 1.6 pad_maximum_fusion.1
  8.2 22.0 %all-gather.1 = bf16[3072,128]{1,0:T(8,128)(2,1)} all-gather(bf16[768,128]{1,0:T(8,128)(2,1)} %param.25), channel_id=3, replica_groups=mesh['rep'=2,'fs_0'=4,'fs_1'=4,'tp'=8] {'fs_0'}, dimensions={0}, use_global_device_ids=true | all-gather | bytes 983040 | tf_op jit(solution)/shard_map/all_gather | solution.py:54
  30.2 0.1 copy.39
  30.3 1.6 broadcast_in_dim.20
  31.9 4.9 %all-to-all-start = ((bf16[8,512,256]{1,2,0:T(8,128)(2,1)}), bf16[8,512,256]{1,2,0:T(8,128)(2,1)S(1)}, u32[]{:S(2)}, u32[]{:S(2)}) async-start(bf16[8,512,256]{1,2,0:T(8,128)(2,1)} %broadcast_in_dim.20), calls=%async_computation | async-start | bytes 4194304 | tf_op jit(solution)/shard_map/all_to_all | solution.py:24
  36.9 23.9 %all-gather = bf16[512,768]{1,0:T(8,128)(2,1)} all-gather(bf16[128,768]{1,0:T(8,128)(2,1)S(1)} %copy-done.3), channel_id=2, replica_groups=mesh['rep'=2,'fs_0'=4,'fs_1'=4,'tp'=8] {'fs_0'}, dimensions={0}, use_global_device_ids=true | all-gather | bytes 983040 | tf_op jit(solution)/shard_map/all_gather | solution.py:54
  61.0 1.1 broadcast_in_dim.21
  62.1 7.0 %all-to-all-start.1 = ((bf16[16,256,128]{1,2,0:T(8,128)(2,1)}), bf16[16,256,128]{1,2,0:T(8,128)(2,1)S(1)}, u32[]{:S(2)}, u32[]{:S(2)}) async-start(bf16[16,256,128]{1,2,0:T(8,128)(2,1)} %broadcast_in_dim.21), calls=%async_computation.1 | async-start | bytes 2097152 | tf_op jit(solution)/shard_map/all_to_all | solution.py:24
  69.1 0.5 multiply_reduce_fusion
  69.6 1.9 fusion.4
  71.6 27.4 %all-gather.6.cloned.1.call-done = bf16[2048,512]{1,0:T(8,128)(2,1)} async-done(((bf16[128,512]{1,0:T(8,128)(2,1)}), bf16[2048,512]{1,0:T(8,128)(2,1)}) %all-gather.6.cloned.1.call-update) | async-done | bytes 2097168 | tf_op jit(solution)/shard_map/all_gather | solution.py:37
  98.9 2.6 %convolution_convert_fusion.3 = bf16[512,256]{1,0:T(8,128)(2,1)S(1)} fusion(bf16[512,2048]{0,1:T(8,128)(2,1)} %fusion.4, bf16[2048,512]{1,0:T(8,128)(2,1)} %all-gather.6.cloned.1.call-done), kind=kOutput, calls=%fused_computation.25 | convolution fusion | flops 537001984 | bytes 3407872 | tf_op jit(solution)/shard_map/dot_general | solution.py:149
  101.6 0.2 add_convert_fusion.2
  101.8 0.2 copy.40
  102.2 0.3 fusion.8
  102.5 0.2 copy.42
  102.7 0.2 copy-done.9
  102.9 0.3 fusion.10
  103.2 0.2 copy.44
  103.4 1.5 fusion.47
  104.9 0.1 slice.191
  105.0 0.1 slice.192
  105.2 0.1 slice.190
  105.3 0.8 slice.194
  106.1 1.0 fusion.57
  108.6 0.2 slice.238
  108.8 0.2 slice.189
  109.9 2.9 %convolution_convert_fusion.2 = bf16[512,256]{1,0:T(8,128)(2,1)S(1)} fusion(bf16[512,2048]{0,1:T(8,128)(2,1)} %fusion.4, bf16[2048,512]{1,0:T(8,128)(2,1)} %all-gather.6.cloned.1.call-done), kind=kOutput, calls=%fused_computation.24 | convolution fusion | flops 537001984 | bytes 3407872 | tf_op jit(solution)/shard_map/dot_general | solution.py:150
  112.9 1.2 fusion.15
  114.1 0.7 convolution_convert_fusion
  114.8 0.1 copy.59
  114.9 28.9 %all_to_all.25 = bf16[8,512,256]{2,1,0:T(8,128)(2,1)S(1)} all-to-all(bf16[8,512,256]{2,1,0:T(8,128)(2,1)S(1)} %bitcast.83), channel_id=1, replica_groups=mesh['rep'=2,'fs_0'=4,'fs_1'=4,'tp'=8] {'tp'}, dimensions={0} | all-to-all | bytes 4194304 | tf_op jit(solution)/shard_map/all_to_all | solution.py:47
  143.9 0.3 convert_reduce_fusion.1
  144.2 0.6 copy-done.2
  144.9 0.1 copy.47
  145.0 1.5 broadcast_in_dim.22
  146.5 6.5 %all-to-all-start.3 = ((bf16[8,512,256]{1,2,0:T(8,128)(2,1)}), bf16[8,512,256]{1,2,0:T(8,128)(2,1)S(1)}, u32[]{:S(2)}, u32[]{:S(2)}) async-start(bf16[8,512,256]{1,2,0:T(8,128)(2,1)} %broadcast_in_dim.22), calls=%async_computation.3 | async-start | bytes 4194304 | tf_op jit(solution)/shard_map/all_to_all | solution.py:24
  153.1 4.0 %copy.49 = bf16[4,4,768,128]{3,2,1,0:T(8,128)(2,1)} copy(bf16[4,4,768,128]{3,2,0,1:T(8,128)(2,1)} %bitcast.93) | data formatting | bytes 6291456 | tf_op jit(solution)/shard_map/transpose | solution.py:58
  157.1 4.7 %copy.50 = bf16[768,16,128]{0,2,1:T(8,128)(2,1)} copy(bf16[768,16,128]{2,0,1:T(8,128)(2,1)} %bitcast.81) | data formatting | bytes 6291456 | tf_op jit(solution)/shard_map/transpose | solution.py:19
  161.8 23.5 %all-gather.8.cloned.1.call-done = bf16[16,128,768]{2,1,0:T(8,128)(2,1)} async-done(((bf16[4,128,768]{2,1,0:T(8,128)(2,1)}), bf16[16,128,768]{2,1,0:T(8,128)(2,1)}) %all-gather.8.cloned.1.call-update) | async-done | bytes 3145744 | tf_op jit(solution)/shard_map/all_gather | solution.py:54
  185.4 3.9 %copy.48 = bf16[4,4,128,768]{3,2,1,0:T(8,128)(2,1)} copy(bf16[4,4,128,768]{3,2,0,1:T(8,128)(2,1)} %bitcast.94) | data formatting | bytes 6291456 | tf_op jit(solution)/shard_map/transpose | solution.py:58
  189.3 0.5 fusion
  189.8 1.9 fusion.2
  191.7 7.6 %convolution_convert_fusion.1 = bf16[512,2048]{1,0:T(8,128)(2,1)S(1)} fusion(bf16[768,2048]{0,1:T(8,128)(2,1)} %bitcast.95, bf16[512,2048]{0,1:T(8,128)(2,1)} %bitcast.101, bf16[2048,768]{1,0:T(8,128)(2,1)} %bitcast.96), kind=kOutput, calls=%fused_computation.12 | convolution fusion | flops 3223453696 | bytes 10485760 | tf_op jit(solution)/shard_map/dot_general | solution.py:177
  199.3 0.1 copy.58
  199.4 28.9 %all_to_all.26 = bf16[8,512,256]{2,1,0:T(8,128)(2,1)S(1)} all-to-all(bf16[8,512,256]{2,1,0:T(8,128)(2,1)S(1)} %bitcast.84), channel_id=1, replica_groups=mesh['rep'=2,'fs_0'=4,'fs_1'=4,'tp'=8] {'tp'}, dimensions={0} | all-to-all | bytes 4194304 | tf_op jit(solution)/shard_map/all_to_all | solution.py:47
  228.3 0.3 convert_reduce_fusion
  228.6 0.8 add_convert_fusion
  (107 shorter events, 2.6 us)
Async XLA Ops:
  6.5 95.6 %copy-start = (bf16[4,64,64]{2,1,0:T(8,128)(2,1)S(1)}, bf16[4,64,64]{2,1,0:T(8,128)(2,1)}, u32[]{:S(2)}) copy-start(bf16[4,64,64]{2,1,0:T(8,128)(2,1)} %param.19) | copy-start | bytes 98308
  6.5 23.6 %copy-start.1 = (bf16[512,256]{1,0:T(8,128)(2,1)S(1)}, bf16[512,256]{1,0:T(8,128)(2,1)}, u32[]{:S(2)}) copy-start(bf16[512,256]{1,0:T(8,128)(2,1)} %param.13) | copy-start | bytes 786436
  6.5 92.4 %all-gather.6.cloned.1.call-start = ((), (), s32[]{:S(2)}) async-start(), calls=%async_computation.5 | async-start | bytes 2228224 | tf_op jit(solution)/shard_map/all_gather | solution.py:37
  8.1 144.9 %all-gather.10.cloned.1.call-start = ((), (), s32[]{:S(2)}) async-start(), calls=%async_computation.7 | async-start | bytes 3932160 | tf_op jit(solution)/shard_map/all_gather | solution.py:54
  31.9 5.0 %copy-start.3 = (bf16[128,768]{1,0:T(8,128)(2,1)S(1)}, bf16[128,768]{1,0:T(8,128)(2,1)}, u32[]{:S(2)}) copy-start(bf16[128,768]{1,0:T(8,128)(2,1)} %param.24) | copy-start | bytes 589828
  31.9 28.9 %copy-start.4 = (bf16[256,128]{1,0:T(8,128)(2,1)S(1)}, bf16[256,128]{1,0:T(8,128)(2,1)}, u32[]{:S(2)}) copy-start(bf16[256,128]{1,0:T(8,128)(2,1)} %param.23) | copy-start | bytes 196612
  31.9 29.0 %copy-start.8 = (f32[256]{0:T(256)S(1)}, f32[256]{0:T(256)}, u32[]{:S(2)}) copy-start(f32[256]{0:T(256)} %param.21) | copy-start | bytes 3076
  31.9 29.0 %copy-start.7 = (bf16[4,256]{1,0:T(4,128)(2,1)S(1)}, bf16[4,256]{1,0:T(4,128)(2,1)}, u32[]{:S(2)}) copy-start(bf16[4,256]{1,0:T(4,128)(2,1)} %param.18) | copy-start | bytes 6148
  31.9 29.0 %all-to-all-start = ((bf16[8,512,256]{1,2,0:T(8,128)(2,1)}), bf16[8,512,256]{1,2,0:T(8,128)(2,1)S(1)}, u32[]{:S(2)}, u32[]{:S(2)}) async-start(bf16[8,512,256]{1,2,0:T(8,128)(2,1)} %broadcast_in_dim.20), calls=%async_computation | async-start | bytes 4194304 | tf_op jit(solution)/shard_map/all_to_all | solution.py:24
  36.9 148.5 %all-gather.8.cloned.1.call-start = ((), (), s32[]{:S(2)}) async-start(), calls=%async_computation.6 | async-start | bytes 3932160 | tf_op jit(solution)/shard_map/all_gather | solution.py:54
  62.1 7.5 %copy-start.5 = (f32[2048]{0:T(1024)S(1)}, f32[2048]{0:T(1024)}, u32[]{:S(2)}) copy-start(f32[2048]{0:T(1024)} %param.14) | copy-start | bytes 24580
  62.1 52.0 %all-to-all-start.1 = ((bf16[16,256,128]{1,2,0:T(8,128)(2,1)}), bf16[16,256,128]{1,2,0:T(8,128)(2,1)S(1)}, u32[]{:S(2)}, u32[]{:S(2)}) async-start(bf16[16,256,128]{1,2,0:T(8,128)(2,1)} %broadcast_in_dim.21), calls=%async_computation.1 | async-start | bytes 2097152 | tf_op jit(solution)/shard_map/all_to_all | solution.py:24
  102.0 0.8 copy-start.9
  143.9 1.0 copy-start.2
  146.5 6.5 %copy-start.6 = (f32[2048]{0:T(1024)S(1)}, f32[2048]{0:T(1024)}, u32[]{:S(2)}) copy-start(f32[2048]{0:T(1024)} %param.15) | copy-start | bytes 24580
  146.5 42.7 %all-to-all-start.3 = ((bf16[8,512,256]{1,2,0:T(8,128)(2,1)}), bf16[8,512,256]{1,2,0:T(8,128)(2,1)S(1)}, u32[]{:S(2)}, u32[]{:S(2)}) async-start(bf16[8,512,256]{1,2,0:T(8,128)(2,1)} %broadcast_in_dim.22), calls=%async_computation.3 | async-start | bytes 4194304 | tf_op jit(solution)/shard_map/all_to_all | solution.py:24
Sparse Core Ops, SparseCore 0:
  9.1 89.7 all-gather.5
  100.7 40.5 all-gather.9
  143.1 42.2 all-gather.7
where the time goes:
time: 240 us; the launch traced here: 236 us
  blocking collectives  104 us (43%)
  waiting for transfers between devices  51 us (21%)
  local copies, waits for them, and re-layouts  22.1 us (9%)
  starting transfers between devices  18.5 us (8%)
  matrix products  14.5 us (6%)
  between operations  13.8 us (6%)
  other arithmetic  12.3 us (5%)
    all_to_all x2, blocking collectives, sent_and_summed(): lax.all_to_all(pieces, axis, split_axis=0, concat_axis=0, tiled=True)  57.9 us
    all_gather x2, blocking collectives, gather_in_order(): pieces = lax.all_gather(pieces, axes[k], axis=0, tiled=True)  45.8 us
    all_gather x1, waiting for transfers between devices, in_one_piece(): lax.all_gather(both, axis, axis=dim, tiled=True)  27.4 us
    all_gather x2, waiting for transfers between devices, gather_in_order(): pieces = lax.all_gather(pieces, axes[k], axis=0, tiled=True)  23.6 us
    all_to_all x3, starting transfers between devices, from_everyone(): return lax.all_to_all(copies, axis, split_axis=0, concat_axis=0, tiled=True)  18.5 us
    transpose x2, local copies, waits for them, and re-layouts, gather_in_order(): pieces.transpose(*turned, *range(len(order), pieces.ndim))  7.91 us
    dot_general x1, matrix products, shards(): jnp.dot(activity, gather_axes(down_projection_weight, FS, (0, 1), 1), pre...  7.59 us
  transfers between devices with their start and end apart: 6, of which 2 were waited for; matrix products, arithmetic and copies ran while one was open for 15% of the time, Pallas kernels for 0%

commit v1 on v0

v1 whole, which is shorter than its diff:
```python
import jax
import jax.numpy as jnp
from jax import lax
from jax.experimental import pallas as pl
from jax.experimental.pallas import tpu as pltpu
from jax.sharding import Mesh
from jax.sharding import PartitionSpec as P

MESH = pl.DeviceIdType.MESH
SEQ_LEN = 128
FS = ("fs_0", "fs_1")
REP_FS = ("rep", "fs_0", "fs_1")
AXES = ("rep", "fs_0", "fs_1", "tp")

EPSILON = 1e-06
DECAY_MULTIPLIER = 8.0
F32 = jnp.float32
BF16 = jnp.bfloat16

ROWS, WIDTH, PARTS, GROUP = 512, 256, 4, 8
PART = ROWS // PARTS
HALF = PART // 2

KINDS = (
    "oy+", "oy-", "oz+", "oz-",
    "ry+", "ry-", "rz+", "rz-",
    "a1z+", "a1z-", "a3z+", "a3z-", "b1y+", "b1y-", "b3y+", "b3y-",
    "a2z+", "a2z-", "b2y+", "b2y-",
    "last",
)


def wrap(value, n):
    return lax.rem(value + n, n)


class Place:
    def __init__(self):
        self.rep, self.z, self.y, self.tp = (lax.axis_index(a) for a in AXES)
        self.whole_z = self.rep * 4 + self.z
        self.x, self.core = self.tp // 2, lax.rem(self.tp, 2)
        self.other = 1 - self.core

    def device(self, x=0, y=0, z=0, flip=False):
        z_there = wrap(self.whole_z + z, 8)
        core = self.other if flip else self.core
        return (z_there // 4, lax.rem(z_there, 4), wrap(self.y + y, 4), wrap(self.x + x, 4) * 2 + core)

    def shard(self, z=0, y=0):
        return wrap(self.z + z, 4) * 4 + wrap(self.y + y, 4)

    def slot(self, x=0, flip=False):
        return wrap(self.x + x, 4) * 2 + (self.other if flip else self.core)


class WeightGather:
    def __init__(self, place, index, own_ref, held, local_sem, send_sem, recv_sems):
        self.p, self.i, self.own, self.held = place, index, own_ref, held
        self.local = pltpu.make_async_copy(own_ref, held.at[place.shard()], local_sem.at[index])
        self.send_sem, self.recv_sems = send_sem.at[index], recv_sems
        self.sent = {}

    def go(self, kind, shard, part, recv_kind=None):
        where = {"y+": dict(y=1), "y-": dict(y=-1), "z+": dict(z=1), "z-": dict(z=-1)}[kind[-2:]]
        view = self.held.at[(self.p.shard(**shard), *part)]
        copy = pltpu.make_async_remote_copy(
            src_ref=view,
            dst_ref=view,
            send_sem=self.send_sem,
            recv_sem=self.recv_sems.at[self.i, KINDS.index(recv_kind or kind)],
            device_id=self.p.device(**where),
            device_id_type=MESH,
        )
        copy.start()
        self.sent[kind] = copy

    def got(self, *kinds):
        for kind in kinds:
            self.sent[kind].wait_recv()

    def start(self):
        self.local.wait()
        for kind in ("oy+", "oy-", "oz+", "oz-"):
            self.go(kind, {}, ())

    def first(self):
        every = slice(None)
        self.got("oy+")
        self.go("ry+", dict(y=-1), (every, 0))
        self.go("a1z+", dict(y=-1), (0,))
        self.go("a1z-", dict(y=-1), (0,))
        self.got("oz+")
        self.go("rz+", dict(z=-1), (every, 0))
        self.go("b1y+", dict(z=-1), (1,))
        self.go("b1y-", dict(z=-1), (1,))
        self.got("oy-")
        self.go("ry-", dict(y=1), (every, 1))
        self.go("a3z+", dict(y=1), (0,))
        self.go("a3z-", dict(y=1), (0,))
        self.got("oz-")
        self.go("rz-", dict(z=1), (every, 1))
        self.go("b3y+", dict(z=1), (1,))
        self.go("b3y-", dict(z=1), (1,))

    def second(self):
        self.got("ry+", "ry-")
        self.go("a2z+", dict(y=2), (0,))
        self.go("a2z-", dict(y=2), (0,))
        self.got("rz+", "rz-")
        self.go("b2y+", dict(z=2), (1,))
        self.go("b2y-", dict(z=2), (1,))
        for n, y in ((1, -1), (3, 1)):
            self.got(f"a{n}z+")
            self.go(f"f{n}z+", dict(z=-1, y=y), (0, 0), "last")
            self.got(f"a{n}z-")
            self.go(f"f{n}z-", dict(z=1, y=y), (0, 1), "last")
        for n, z in ((1, -1), (3, 1)):
            self.got(f"b{n}y+")
            self.go(f"g{n}y+", dict(z=z, y=-1), (1, 0), "last")
            self.got(f"b{n}y-")
            self.go(f"g{n}y-", dict(z=z, y=1), (1, 1), "last")

    def third(self):
        self.got("a2z+")
        self.go("f2z+", dict(z=-1, y=2), (0, 0), "last")
        self.got("a2z-")
        self.go("f2z-", dict(z=1, y=2), (0, 1), "last")
        self.got("b2y+")
        self.go("g2y+", dict(z=2, y=-1), (1, 0), "last")
        self.got("b2y-")
        self.go("g2y-", dict(z=2, y=1), (1, 1), "last")

    def bytes_of(self, shards, sem):
        view = self.held.at[pl.ds(0, shards)]
        pltpu.make_async_copy(view, view, sem).wait()

    def finish(self):
        self.bytes_of(3, self.recv_sems.at[self.i, KINDS.index("last")])

    def drain(self):
        self.bytes_of(15, self.send_sem)


class TokenGather:
    def __init__(self, place, index, held, start, rows, send_sems, recv_sems):
        self.p, self.held, self.start, self.rows = place, held, start, rows
        self.send_sem, self.recv_sems = send_sems.at[index], recv_sems.at[index]
        self.sent = {}

    def go(self, name, sem, slot, device, start=0, rows=None):
        view = self.held.at[slot, pl.ds(self.start + start, rows or self.rows)]
        copy = pltpu.make_async_remote_copy(
            src_ref=view,
            dst_ref=view,
            send_sem=self.send_sem,
            recv_sem=self.recv_sems.at[sem],
            device_id=device,
            device_id_type=MESH,
        )
        copy.start()
        self.sent[name] = copy

    def slots_of(self, slots, sem):
        view = self.held.at[pl.ds(0, slots), pl.ds(self.start, self.rows)]
        pltpu.make_async_copy(view, view, sem).wait()

    def begin(self):
        p = self.p
        self.go("o+", 0, p.slot(), p.device(x=1))
        self.go("o-", 1, p.slot(), p.device(x=-1))
        self.go("p0", 3, p.slot(), p.device(flip=True))

    def near(self):
        p, half = self.p, self.rows // 2
        self.sent["o+"].wait_recv()
        self.go("f+", 2, p.slot(x=-1), p.device(x=1), 0, half)
        self.go("p1", 3, p.slot(x=-1), p.device(flip=True))
        self.sent["o-"].wait_recv()
        self.go("f-", 2, p.slot(x=1), p.device(x=-1), half, half)
        self.go("p3", 3, p.slot(x=1), p.device(flip=True))

    def far(self):
        p = self.p
        self.slots_of(1, self.recv_sems.at[2])
        self.go("p2", 3, p.slot(x=2), p.device(flip=True))

    def finish(self):
        self.slots_of(4, self.recv_sems.at[3])

    def drain(self):
        self.slots_of(7, self.send_sem)


class TokenSum:
    def __init__(self, place, index, part, terms, from_core, chip, near, last, send_sems, recv_sems):
        self.p, self.part, self.rows = place, part, pl.ds(part * PART, PART)
        self.terms, self.from_core, self.chip, self.near, self.last = terms, from_core, chip, near, last
        self.send_sem, self.recv_sems = send_sems.at[index], recv_sems.at[index]
        self.sent = {}

    def go(self, name, sem, src, dst, device):
        copy = pltpu.make_async_remote_copy(
            src_ref=src,
            dst_ref=dst,
            send_sem=self.send_sem,
            recv_sem=self.recv_sems.at[sem],
            device_id=device,
            device_id_type=MESH,
        )
        copy.start()
        self.sent[name] = copy

    def half(self, h):
        return pl.ds(self.part * PART + h * HALF, HALF)

    def begin(self):
        p = self.p
        self.go("d", 0, self.terms.at[:, p.other, self.rows], self.from_core.at[:, self.rows], p.device(flip=True))

    def chip_sum(self, x):
        p = self.p
        there = wrap(p.x + x, 4)
        return self.terms[there, p.core, self.rows].astype(F32) + self.from_core[there, self.rows].astype(F32)

    def cores(self):
        p, chip = self.p, self.chip
        self.sent["d"].wait_recv()
        right, left, far = wrap(p.x + 1, 4), wrap(p.x - 1, 4), wrap(p.x + 2, 4)
        chip[far, self.rows] = self.chip_sum(2).astype(BF16)
        self.go("h+", 1, chip.at[far, self.half(0)], self.near.at[0, self.half(0)], p.device(x=1))
        self.go("h-", 2, chip.at[far, self.half(1)], self.near.at[1, self.half(1)], p.device(x=-1))
        chip[right, self.rows] = self.chip_sum(1).astype(BF16)
        self.go("e+", 3, chip.at[right, self.half(1)], self.last.at[0, self.half(1)], p.device(x=1))
        chip[left, self.rows] = self.chip_sum(-1).astype(BF16)
        self.go("e-", 3, chip.at[left, self.half(0)], self.last.at[1, self.half(0)], p.device(x=-1))

    def ring(self):
        p, chip = self.p, self.chip
        for name, x, h, side in (("h+", 1, 0, 0), ("h-", -1, 1, 1)):
            there = wrap(p.x + x, 4)
            rows = self.half(h)
            self.sent[name].wait_recv()
            total = chip[there, rows].astype(F32) + self.near[side, rows].astype(F32)
            self.near[side, rows] = total.astype(BF16)
            self.go("e2" + name, 3, self.near.at[side, rows], self.last.at[side, rows], p.device(x=x))

    def finish(self, base):
        both = self.last.at[:, self.rows]
        pltpu.make_async_copy(both, both, self.recv_sems.at[3]).wait()
        total = self.chip_sum(0) + (self.last[0, self.rows].astype(F32) + self.last[1, self.rows].astype(F32))
        return (base.astype(F32) + total).astype(BF16)

    def drain(self):
        view = self.terms.at[:, 0, self.rows]
        part = self.chip.at[pl.ds(0, 3), self.rows]
        pltpu.make_async_copy(view, view, self.send_sem).wait()
        pltpu.make_async_copy(part, part, self.send_sem).wait()


def norm_rows(held, rows, gain_ref, normed):
    total = jnp.zeros((PART, 1), F32)
    for k in range(GROUP):
        piece = held[k, rows].astype(F32)
        total = total + jnp.sum(piece * piece, axis=-1, keepdims=True)
    inverse = lax.rsqrt(total * (1.0 / (GROUP * WIDTH)) + EPSILON)
    for k in range(GROUP):
        columns = slice(k * WIDTH, (k + 1) * WIDTH)
        piece = held[k, rows].astype(F32) * inverse * gain_ref[:, columns]
        normed[rows, columns] = piece.astype(BF16)


def block_diagonal(matrix_ref, out_ref, offset):
    blocks, size, _ = matrix_ref.shape
    row = lax.broadcasted_iota(jnp.int32, (size, blocks * size), 0)
    column = lax.broadcasted_iota(jnp.int32, (size, blocks * size), 1)
    for b in range(blocks):
        select = (column == row + b * size).astype(F32).astype(BF16)
        spread = jnp.dot(matrix_ref[b], select, preferred_element_type=F32)
        out_ref[b * size : (b + 1) * size, offset : offset + blocks * size] = spread.astype(BF16)


def shifted(values, by, row, fill):
    return jnp.where(row >= by, pltpu.roll(values, by, 0), fill)


def mixer_rows(values, gates, offsets, taps, maps, rate):
    channels = values.shape[1]
    row = lax.broadcasted_iota(jnp.int32, values.shape, 0)
    wide = values.astype(F32)
    reach = taps.shape[0]
    total = taps[0:1] * shifted(wide, reach - 1, row, 0.0)
    for k in range(1, reach):
        by = reach - 1 - k
        total = total + taps[k : k + 1] * (shifted(wide, by, row, 0.0) if by else wide)
    conved = total.astype(BF16)
    both = jax.nn.sigmoid(jnp.dot(conved, maps, preferred_element_type=F32))
    decay = rate * both[:, :channels] + offsets
    factor = jnp.exp(decay)
    twice = 2.0 * decay
    small = -twice * (1.0 + twice * (0.5 + twice * (1.0 / 6.0 + twice * (1.0 / 24.0))))
    lost = jnp.where(twice > -0.03, small, 1.0 - factor * factor)
    state = jnp.sqrt(lost) * both[:, channels:] * conved.astype(F32)
    by = 1
    while by < SEQ_LEN:
        state = factor * shifted(state, by, row, 0.0) + state
        if 2 * by < SEQ_LEN:
            factor = factor * shifted(factor, by, row, 1.0)
        by *= 2
    gate = gates.astype(F32)
    gelu = 0.5 * gate * (1.0 + lax.erf(gate * (0.5**0.5)))
    return (state * gelu).astype(BF16)


def kernel(
    stream_ref, gain1_ref, gain2_ref, input_ref, gate_ref, taps_ref, decay_ref, inmap_ref, param_ref, offset_hbm,
    output_ref, up_ref, down_ref,
    out_ref,
    w_input, w_gate, w_output, w_up, w_down,
    held1, held2, normed, values, gates, offsets, mixed, activity, maps,
    terms1, core1, chip1, near1, last1, terms2, core2, chip2, near2, last2,
    local_sem, wsend, wrecv, tsend, trecv,
):
    p = Place()
    weights = [
        WeightGather(p, i, own, held, local_sem, wsend, wrecv)
        for i, (own, held) in enumerate(
            (
                (input_ref, w_input),
                (gate_ref, w_gate),
                (output_ref, w_output),
                (up_ref, w_up),
                (down_ref, w_down),
            )
        )
    ]
    own_stream = pltpu.make_async_copy(stream_ref, held1.at[p.tp], local_sem.at[5])
    own_offsets = pltpu.make_async_copy(offset_hbm, offsets, local_sem.at[6])
    for w in weights[:2]:
        w.local.start()
    own_stream.start()
    for w in weights[2:]:
        w.local.start()
    own_offsets.start()

    barrier = pltpu.get_barrier_semaphore()
    greeted = [dict(x=1), dict(x=-1), dict(y=1), dict(y=-1), dict(z=1), dict(z=-1), dict(flip=True)]
    for where in greeted:
        pl.semaphore_signal(barrier, inc=1, device_id=p.device(**where), device_id_type=MESH)
    pl.semaphore_wait(barrier, len(greeted))

    gather1 = TokenGather(p, 0, held1, 0, ROWS, tsend, trecv)
    gather2 = [TokenGather(p, 1 + c, held2, c * PART, PART, tsend, trecv) for c in range(PARTS)]
    sum1 = [
        TokenSum(p, 1 + PARTS + c, c, terms1, core1, chip1, near1, last1, tsend, trecv) for c in range(PARTS)
    ]
    sum2 = [
        TokenSum(p, 1 + 2 * PARTS + c, c, terms2, core2, chip2, near2, last2, tsend, trecv) for c in range(PARTS)
    ]
    w_in, w_g, w_out, w_u, w_d = weights

    w_in.start()
    w_g.start()
    own_stream.wait()
    gather1.begin()
    w_out.start()
    block_diagonal(decay_ref, maps, 0)
    block_diagonal(inmap_ref, maps, WIDTH)
    parameter = -param_ref[...]
    rate = -DECAY_MULTIPLIER * (jnp.maximum(parameter, 0.0) + jnp.log1p(jnp.exp(-jnp.abs(parameter))))
    w_in.first()
    w_g.first()
    gather1.near()
    w_in.second()
    w_g.second()
    w_out.first()
    w_u.start()
    gather1.far()
    w_in.third()
    w_g.third()
    w_out.second()
    gather1.finish()

    @pl.loop(0, PARTS)
    def _(c):
        norm_rows(held1, pl.ds(pl.multiple_of(c * PART, PART), PART), gain1_ref, normed)

    w_in.finish()
    w_g.finish()

    tall = ROWS // 2

    @pl.loop(0, 2)
    def _(m):
        rows = pl.ds(pl.multiple_of(m * tall, tall), tall)
        columns = normed[rows, :]
        full = w_input[...].reshape(GROUP * WIDTH, WIDTH)
        values[rows, :] = jnp.dot(columns, full, preferred_element_type=F32).astype(BF16)
        full = w_gate[...].reshape(GROUP * WIDTH, WIDTH)
        gates[rows, :] = jnp.dot(columns, full, preferred_element_type=F32).astype(BF16)

    w_out.third()
    w_u.first()
    own_offsets.wait()
    taps = taps_ref[...].astype(F32)

    def columns_of(held, j, depth):
        pair = held[pl.ds(2 * j, 2)].reshape(2, depth, 128)
        return jnp.concatenate([pair[0], pair[1]], axis=1)

    def mix(c):
        rows = pl.ds(c * PART, PART)
        mixed[rows, :] = mixer_rows(values[rows, :], gates[rows, :], offsets[rows, :], taps, maps[...], rate)

    def project(c, source, held, depth, terms):
        rows = pl.ds(c * PART, PART)

        @pl.loop(0, GROUP)
        def _(j):
            total = jnp.dot(source[rows, :], columns_of(held, j, depth), preferred_element_type=F32)
            terms[j // 2, lax.rem(j, 2), rows] = total.astype(BF16)

    def middle_of(c):
        rows = pl.ds(c * PART, PART)
        held2[p.tp, rows] = sum1[c].finish(held1[p.tp, rows])
        gather2[c].begin()

    def raise_rows(c):
        rows = pl.ds(c * PART, PART)
        norm_rows(held2, rows, gain2_ref, normed)

    mix(0)
    w_out.finish()
    project(0, mixed, w_output, WIDTH, terms1)
    sum1[0].begin()
    w_d.start()
    w_u.second()
    mix(1)
    project(1, mixed, w_output, WIDTH, terms1)
    sum1[1].begin()
    sum1[0].cores()
    mix(2)
    project(2, mixed, w_output, WIDTH, terms1)
    sum1[2].begin()
    sum1[1].cores()
    sum1[0].ring()
    w_u.third()
    mix(3)
    project(3, mixed, w_output, WIDTH, terms1)
    sum1[3].begin()
    sum1[2].cores()
    sum1[1].ring()
    middle_of(0)
    w_d.first()
    sum1[3].cores()
    sum1[2].ring()
    middle_of(1)
    gather2[0].near()
    sum1[3].ring()
    middle_of(2)
    gather2[1].near()
    gather2[0].far()
    w_d.second()
    middle_of(3)
    gather2[2].near()
    gather2[1].far()
    gather2[0].finish()
    raise_rows(0)
    gather2[3].near()
    gather2[2].far()
    gather2[1].finish()
    raise_rows(1)
    gather2[3].far()
    gather2[2].finish()
    raise_rows(2)
    gather2[3].finish()
    raise_rows(3)
    w_d.third()
    w_u.finish()

    hidden = w_up.shape[-1]

    def lift(c):
        rows = pl.ds(c * PART, PART)
        columns = normed[rows, :]
        for n in range(hidden // WIDTH):
            some = slice(n * WIDTH, (n + 1) * WIDTH)
            full = w_up[:, :, :, :, some].reshape(GROUP * WIDTH, WIDTH)
            raised = jnp.maximum(jnp.dot(columns, full, preferred_element_type=F32), 0.0)
            activity[rows, some] = (raised * raised).astype(BF16)

    for c in range(PARTS):
        lift(c)
    w_d.finish()

    def last_of(c):
        rows = pl.ds(c * PART, PART)
        out_ref[rows, :] = sum2[c].finish(held2[p.tp, rows])

    for c in range(PARTS + 3):
        if c < PARTS:
            project(c, activity, w_down, hidden, terms2)
            sum2[c].begin()
        if 0 <= c - 1 < PARTS:
            sum2[c - 1].cores()
        if 0 <= c - 2 < PARTS:
            sum2[c - 2].ring()
        if 0 <= c - 3 < PARTS:
            last_of(c - 3)

    for w in weights:
        w.drain()
    for event in (gather1, *gather2, *sum1, *sum2):
        event.drain()


def quarters(weight):
    rows, columns = weight.shape
    return weight.reshape(2, 2, rows // 4, columns)


def shards(
    stream,
    recurrent_norm_gain,
    feedforward_norm_gain,
    recurrent_input_weight,
    output_gate_weight,
    causal_filter_weight,
    decay_gate_matrix,
    input_gate_matrix,
    channel_decay_param,
    token_decay_offset,
    recurrent_output_weight,
    up_projection_weight,
    down_projection_weight,
):
    cut = [
        quarters(w)
        for w in (
            recurrent_input_weight,
            output_gate_weight,
            recurrent_output_weight,
            up_projection_weight,
            down_projection_weight,
        )
    ]
    hidden = up_projection_weight.shape[1]
    far, near = pl.BlockSpec(memory_space=pltpu.HBM), pl.BlockSpec(memory_space=pltpu.VMEM)
    sums = [
        pltpu.VMEM((4, 2, ROWS, WIDTH), BF16),
        pltpu.VMEM((4, ROWS, WIDTH), BF16),
        pltpu.VMEM((4, ROWS, WIDTH), BF16),
        pltpu.VMEM((2, ROWS, WIDTH), BF16),
        pltpu.VMEM((2, ROWS, WIDTH), BF16),
    ]
    events = 1 + 3 * PARTS
    return pl.pallas_call(
        kernel,
        out_shape=jax.ShapeDtypeStruct(stream.shape, stream.dtype),
        in_specs=[far, near, near, far, far, near, near, near, near, far, far, far, far],
        out_specs=near,
        scratch_shapes=[
            *[pltpu.VMEM((16, *w.shape), BF16) for w in cut],
            pltpu.VMEM((GROUP, ROWS, WIDTH), BF16),
            pltpu.VMEM((GROUP, ROWS, WIDTH), BF16),
            pltpu.VMEM((ROWS, GROUP * WIDTH), BF16),
            pltpu.VMEM((ROWS, WIDTH), BF16),
            pltpu.VMEM((ROWS, WIDTH), BF16),
            pltpu.VMEM((ROWS, WIDTH), F32),
            pltpu.VMEM((ROWS, WIDTH), BF16),
            pltpu.VMEM((ROWS, hidden), BF16),
            pltpu.VMEM((WIDTH, 2 * WIDTH), BF16),
            *sums,
            *sums,
            pltpu.SemaphoreType.DMA((7,)),
            pltpu.SemaphoreType.DMA((5,)),
            pltpu.SemaphoreType.DMA((5, len(KINDS))),
            pltpu.SemaphoreType.DMA((events,)),
            pltpu.SemaphoreType.DMA((events, 4)),
        ],
        compiler_params=pltpu.CompilerParams(
            collective_id=0, has_side_effects=True, vmem_limit_bytes=60 * 1024 * 1024
        ),
    )(
        stream,
        recurrent_norm_gain.reshape(1, -1),
        feedforward_norm_gain.reshape(1, -1),
        cut[0],
        cut[1],
        causal_filter_weight,
        decay_gate_matrix,
        input_gate_matrix,
        channel_decay_param.reshape(1, -1),
        token_decay_offset,
        cut[2],
        cut[3],
        cut[4],
    )


def solution(mesh):
    split = Mesh(
        mesh.devices.reshape(mesh.shape["rep"], 4, 4, mesh.shape["tp"]),
        AXES,
    )
    placed = (
        P(REP_FS, "tp"),
        P(),
        P(),
        P(FS, "tp"),
        P(FS, "tp"),
        P(None, "tp"),
        P("tp", None, None),
        P("tp", None, None),
        P("tp"),
        P(REP_FS, "tp"),
        P("tp", FS),
        P(FS, "tp"),
        P("tp", FS),
    )
    return jax.shard_map(
        shards, mesh=split, in_specs=placed, out_specs=P(REP_FS, "tp"), check_vma=False
    )
```

time: 240 us -> 93.1 us (0.39); the launches traced: 236 us -> 92.3 us
  blocking collectives: 104 us -> 0 us
  Pallas kernels: 0 us -> 90.6 us
  waiting for transfers between devices: 51 us -> 0 us
  local copies, waits for them, and re-layouts: 22.1 us -> 1.67 us
  starting transfers between devices: 18.5 us -> 0 us
  matrix products: 14.5 us -> 0 us
  between operations: 13.8 us -> 0.01 us
  other arithmetic: 12.3 us -> 0 us
    pallas_call x0 -> x1, Pallas kernels: none -> 90.6 us  [shards(): pl.pallas_call(kernel, out_shape=jax.ShapeDtypeStruct(stream.shape, strea...]
    all_to_all x2 -> x0, blocking collectives: 57.9 us -> none  [sent_and_summed(): lax.all_to_all(pieces, axis, split_axis=0, concat_axis=0, tiled=True)]
    all_gather x3 -> x0, waiting for transfers between devices: 50.9 us -> none  [the longest x1 27.4 us: in_one_piece(): lax.all_gather(both, axis, axis=dim, tiled=True)]
    all_gather x2 -> x0, blocking collectives: 45.8 us -> none  [gather_in_order(): pieces = lax.all_gather(pieces, axes[k], axis=0, tiled=True)]
    all_to_all x3 -> x0, starting transfers between devices: 18.5 us -> none  [from_everyone(): return lax.all_to_all(copies, axis, split_axis=0, concat_axis=0, tiled=True)]
    dot_general x6 -> x0, matrix products: 14.5 us -> none  [the longest x1 7.59 us: shards(): jnp.dot(activity, gather_axes(down_projection_weight, FS, (0, 1), 1), pre...]
    transpose x3 -> x0, local copies, waits for them, and re-layouts: 12.6 us -> none  [the longest x2 7.91 us: gather_in_order(): pieces.transpose(*turned, *range(len(order), pieces.ndim))]
    convert_element_type x6 -> x0, other arithmetic: 6.02 us -> none  [the longest x2 3.81 us: norm_rows(): return (widened * inverse * gain).astype(jnp.bfloat16)]
  transfers between devices with their start and end apart: 6 -> 0, of which waited for: 2 -> 0; matrix products, arithmetic and copies ran while one was open for 15% -> 0% of each run, Pallas kernels for 0% -> 0%
where the time goes in v1:
time: 93.1 us; the launch traced here: 92.3 us
  Pallas kernels  90.6 us (97%)
  local copies, waits for them, and re-layouts  1.67 us (2%)
    pallas_call x1, Pallas kernels, shards(): pl.pallas_call(kernel, out_shape=jax.ShapeDtypeStruct(stream.shape, strea...  90.6 us

profile of v1, /device:TPU:4, one launch (start us, length us, event | category | flops | bytes accessed | tf_op | source)
XLA Modules:
  0.0 92.3 jit_solution(13144198143931869277)
XLA Ops:
  0.0 90.6 %shard_map.127 = bf16[512,256]{1,0:T(8,128)(2,1)} custom-call(bf16[512,256]{1,0:T(8,128)(2,1)} %stream_ref.1, f32[1,2048]{1,0:T(1,128)} %bitcast.13, f32[1,2048]{1,0:T(1,128)} %bitcast.14, bf16[2,2,32,256]{3,2,1,0:T(8,128)(2,1)} %bitcast.10, bf16[2,2,32,256]{3,2,1,0:T(8,128)(2,1)} %bitcast.11, bf16[4,256]{1,0:T(4,128)(2,1)} %taps_ref.1, ...), custom_call_target="tpu_custom_call" | custom-call | tf_op jit(solution)/shard_map/pallas_call | solution.py:556
  90.6 1.7 %copy.15 = bf16[512,256]{1,0:T(8,128)(2,1)} copy(bf16[512,256]{1,0:T(8,128)(2,1)} %shard_map.127) | data formatting | bytes 524288

commit v2 on v1

--- a/solution.py
+++ b/solution.py
@@ -1,3 +1,5 @@
+import functools
+
 import jax
 import jax.numpy as jnp
 from jax import lax
@@ -21,13 +23,31 @@
 PART = ROWS // PARTS
 HALF = PART // 2
 
-KINDS = (
-    "oy+", "oy-", "oz+", "oz-",
-    "ry+", "ry-", "rz+", "rz-",
-    "a1z+", "a1z-", "a3z+", "a3z-", "b1y+", "b1y-", "b3y+", "b3y-",
-    "a2z+", "a2z-", "b2y+", "b2y-",
-    "last",
-)
+EVERY = slice(None)
+STEPS = {
+    "S": ((), (("oy+", 0, 0, ()), ("oy-", 0, 0, ()), ("oz+", 0, 0, ()), ("oz-", 0, 0, ()))),
+    "a": (("oy+",), (("ry+", 0, -1, (EVERY, 0)), ("a1z+", 0, -1, (0,)), ("a1z-", 0, -1, (0,)))),
+    "b": (("oz+",), (("rz+", -1, 0, (EVERY, 0)), ("b1y+", -1, 0, (1,)), ("b1y-", -1, 0, (1,)))),
+    "c": (("oy-",), (("ry-", 0, 1, (EVERY, 1)), ("a3z+", 0, 1, (0,)), ("a3z-", 0, 1, (0,)))),
+    "d": (("oz-",), (("rz-", 1, 0, (EVERY, 1)), ("b3y+", 1, 0, (1,)), ("b3y-", 1, 0, (1,)))),
+    "e": (("ry+", "ry-"), (("a2z+", 0, 2, (0,)), ("a2z-", 0, 2, (0,)))),
+    "f": (("rz+", "rz-"), (("b2y+", 2, 0, (1,)), ("b2y-", 2, 0, (1,)))),
+    "g": (("a1z+",), (("f1z+", -1, -1, (0, 0)),)),
+    "h": (("a1z-",), (("f1z-", 1, -1, (0, 1)),)),
+    "i": (("a3z+",), (("f3z+", -1, 1, (0, 0)),)),
+    "j": (("a3z-",), (("f3z-", 1, 1, (0, 1)),)),
+    "k": (("b1y+",), (("g1y+", -1, -1, (1, 0)),)),
+    "l": (("b1y-",), (("g1y-", -1, 1, (1, 1)),)),
+    "m": (("b3y+",), (("g3y+", 1, -1, (1, 0)),)),
+    "n": (("b3y-",), (("g3y-", 1, 1, (1, 1)),)),
+    "o": (("a2z+",), (("f2z+", -1, 2, (0, 0)),)),
+    "p": (("a2z-",), (("f2z-", 1, 2, (0, 1)),)),
+    "q": (("b2y+",), (("g2y+", 2, -1, (1, 0)),)),
+    "r": (("b2y-",), (("g2y-", 2, 1, (1, 1)),)),
+}
+SENT = [message[0] for _, sends in STEPS.values() for message in sends]
+LAST = [name for name in SENT if name[0] in "fg"]
+KINDS = [name for name in SENT if name not in LAST] + ["last"]
 
 
 def wrap(value, n):
@@ -60,75 +80,28 @@
         self.send_sem, self.recv_sems = send_sem.at[index], recv_sems
         self.sent = {}
 
-    def go(self, kind, shard, part, recv_kind=None):
+    def go(self, kind, z, y, part):
         where = {"y+": dict(y=1), "y-": dict(y=-1), "z+": dict(z=1), "z-": dict(z=-1)}[kind[-2:]]
-        view = self.held.at[(self.p.shard(**shard), *part)]
+        view = self.held.at[(self.p.shard(z, y), *part)]
         copy = pltpu.make_async_remote_copy(
             src_ref=view,
             dst_ref=view,
             send_sem=self.send_sem,
-            recv_sem=self.recv_sems.at[self.i, KINDS.index(recv_kind or kind)],
+            recv_sem=self.recv_sems.at[self.i, KINDS.index("last" if kind in LAST else kind)],
             device_id=self.p.device(**where),
             device_id_type=MESH,
         )
         copy.start()
         self.sent[kind] = copy
 
-    def got(self, *kinds):
-        for kind in kinds:
+    def step(self, name):
+        if name == "S":
+            self.local.wait()
+        waits, sends = STEPS[name]
+        for kind in waits:
             self.sent[kind].wait_recv()
-
-    def start(self):
-        self.local.wait()
-        for kind in ("oy+", "oy-", "oz+", "oz-"):
-            self.go(kind, {}, ())
-
-    def first(self):
-        every = slice(None)
-        self.got("oy+")
-        self.go("ry+", dict(y=-1), (every, 0))
-        self.go("a1z+", dict(y=-1), (0,))
-        self.go("a1z-", dict(y=-1), (0,))
-        self.got("oz+")
-        self.go("rz+", dict(z=-1), (every, 0))
-        self.go("b1y+", dict(z=-1), (1,))
-        self.go("b1y-", dict(z=-1), (1,))
-        self.got("oy-")
-        self.go("ry-", dict(y=1), (every, 1))
-        self.go("a3z+", dict(y=1), (0,))
-        self.go("a3z-", dict(y=1), (0,))
-        self.got("oz-")
-        self.go("rz-", dict(z=1), (every, 1))
-        self.go("b3y+", dict(z=1), (1,))
-        self.go("b3y-", dict(z=1), (1,))
-
-    def second(self):
-        self.got("ry+", "ry-")
-        self.go("a2z+", dict(y=2), (0,))
-        self.go("a2z-", dict(y=2), (0,))
-        self.got("rz+", "rz-")
-        self.go("b2y+", dict(z=2), (1,))
-        self.go("b2y-", dict(z=2), (1,))
-        for n, y in ((1, -1), (3, 1)):
-            self.got(f"a{n}z+")
-            self.go(f"f{n}z+", dict(z=-1, y=y), (0, 0), "last")
-            self.got(f"a{n}z-")
-            self.go(f"f{n}z-", dict(z=1, y=y), (0, 1), "last")
-        for n, z in ((1, -1), (3, 1)):
-            self.got(f"b{n}y+")
-            self.go(f"g{n}y+", dict(z=z, y=-1), (1, 0), "last")
-            self.got(f"b{n}y-")
-            self.go(f"g{n}y-", dict(z=z, y=1), (1, 1), "last")
-
-    def third(self):
-        self.got("a2z+")
-        self.go("f2z+", dict(z=-1, y=2), (0, 0), "last")
-        self.got("a2z-")
-        self.go("f2z-", dict(z=1, y=2), (0, 1), "last")
-        self.got("b2y+")
-        self.go("g2y+", dict(z=2, y=-1), (1, 0), "last")
-        self.got("b2y-")
-        self.go("g2y-", dict(z=2, y=1), (1, 1), "last")
+        for message in sends:
+            self.go(*message)
 
     def bytes_of(self, shards, sem):
         view = self.held.at[pl.ds(0, shards)]
@@ -170,14 +143,16 @@
         self.go("o-", 1, p.slot(), p.device(x=-1))
         self.go("p0", 3, p.slot(), p.device(flip=True))
 
-    def near(self):
+    def near(self, sign):
         p, half = self.p, self.rows // 2
-        self.sent["o+"].wait_recv()
-        self.go("f+", 2, p.slot(x=-1), p.device(x=1), 0, half)
-        self.go("p1", 3, p.slot(x=-1), p.device(flip=True))
-        self.sent["o-"].wait_recv()
-        self.go("f-", 2, p.slot(x=1), p.device(x=-1), half, half)
-        self.go("p3", 3, p.slot(x=1), p.device(flip=True))
+        if sign == "+":
+            self.sent["o+"].wait_recv()
+            self.go("f+", 2, p.slot(x=-1), p.device(x=1), 0, half)
+            self.go("p1", 3, p.slot(x=-1), p.device(flip=True))
+        else:
+            self.sent["o-"].wait_recv()
+            self.go("f-", 2, p.slot(x=1), p.device(x=-1), half, half)
+            self.go("p3", 3, p.slot(x=1), p.device(flip=True))
 
     def far(self):
         p = self.p
@@ -234,15 +209,14 @@
         chip[left, self.rows] = self.chip_sum(-1).astype(BF16)
         self.go("e-", 3, chip.at[left, self.half(0)], self.last.at[1, self.half(0)], p.device(x=-1))
 
-    def ring(self):
-        p, chip = self.p, self.chip
-        for name, x, h, side in (("h+", 1, 0, 0), ("h-", -1, 1, 1)):
-            there = wrap(p.x + x, 4)
-            rows = self.half(h)
-            self.sent[name].wait_recv()
-            total = chip[there, rows].astype(F32) + self.near[side, rows].astype(F32)
-            self.near[side, rows] = total.astype(BF16)
-            self.go("e2" + name, 3, self.near.at[side, rows], self.last.at[side, rows], p.device(x=x))
+    def ring(self, sign):
+        p = self.p
+        name, x, side = ("h+", 1, 0) if sign == "+" else ("h-", -1, 1)
+        rows = self.half(side)
+        self.sent[name].wait_recv()
+        total = self.chip[wrap(p.x + x, 4), rows].astype(F32) + self.near[side, rows].astype(F32)
+        self.near[side, rows] = total.astype(BF16)
+        self.go("e2" + sign, 3, self.near.at[side, rows], self.last.at[side, rows], p.device(x=x))
 
     def finish(self, base):
         both = self.last.at[:, self.rows]
@@ -311,16 +285,33 @@
     return (state * gelu).astype(BF16)
 
 
+ORDER = (
+    "GS 0S 1S 2S", "X 0a 0b 0c", "0d 1a 1b 1c", "1d 2a 2b 2c", "2d 0g 0h 0l", "G+ G- 0e 0j",
+    "0k 0f 0i 0m", "0n 1g 1h 1l", "1e 1j 1k 1f", "1i 1m 1n 2g", "2h 2l 2e 2j", "2k GB 2f 2i",
+    "2m 2n 0o 0p", "0q 0r GF N0", "3S N1 N2 1o", "1p 1q 1r N3", "2o 2p 2q 2r", "0F 4S 3a 3b",
+    "1F I0 2F I1", "3c 3d M0 M1", "M2 M3 P0 P1", "P2 P3 4a 4b", "K0 K1 K2 3h", "3l K3 3g 4d",
+    "4c R0+ R0- 3k", "R1+ R1- 3e 3f", "R2+ R2- 3i 3j", "3m 3n R3+ R3-", "4g 4h 4l L0", "L1 4k L2 L3",
+    "4f 4n 4m A0+", "A0- 4e 4i 4j", "A1+ A1- A2+ A2-", "3o 3p 3q 3r", "A3+ A3- B0 B1", "B2 Q0 Q1 B3",
+    "4o 4p 4q 4r", "Q2 Q3 3F U0", "U1 U2 4F U3", "V0 V1 V2 V3", "k0 k1 k2 k3", "r0+ r0- r1+ r1-",
+    "r2+ r2- r3+ r3-", "l0 l1 l2 l3",
+)
+
+
 def kernel(
-    stream_ref, gain1_ref, gain2_ref, input_ref, gate_ref, taps_ref, decay_ref, inmap_ref, param_ref, offset_hbm,
+    stream_ref, gain1_hbm, gain2_hbm, input_ref, gate_ref, taps_hbm, decay_hbm, inmap_hbm, param_hbm, offset_hbm,
     output_ref, up_ref, down_ref,
-    out_ref,
+    out_hbm,
     w_input, w_gate, w_output, w_up, w_down,
     held1, held2, normed, values, gates, offsets, mixed, activity, maps,
     terms1, core1, chip1, near1, last1, terms2, core2, chip2, near2, last2,
-    local_sem, wsend, wrecv, tsend, trecv,
+    gain1, gain2, taps_ref, decay_ref, inmap_ref, param_ref, rate_ref, out_ref,
+    local_sem, out_sem, wsend, wrecv, tsend, trecv,
 ):
     p = Place()
+    barrier = pltpu.get_barrier_semaphore()
+    greeted = [dict(x=1), dict(x=-1), dict(y=1), dict(y=-1), dict(z=1), dict(z=-1), dict(flip=True)]
+    for where in greeted:
+        pl.semaphore_signal(barrier, inc=1, device_id=p.device(**where), device_id_type=MESH)
     weights = [
         WeightGather(p, i, own, held, local_sem, wsend, wrecv)
         for i, (own, held) in enumerate(
@@ -334,18 +325,22 @@
         )
     ]
     own_stream = pltpu.make_async_copy(stream_ref, held1.at[p.tp], local_sem.at[5])
-    own_offsets = pltpu.make_async_copy(offset_hbm, offsets, local_sem.at[6])
-    for w in weights[:2]:
-        w.local.start()
-    own_stream.start()
-    for w in weights[2:]:
-        w.local.start()
-    own_offsets.start()
-
-    barrier = pltpu.get_barrier_semaphore()
-    greeted = [dict(x=1), dict(x=-1), dict(y=1), dict(y=-1), dict(z=1), dict(z=-1), dict(flip=True)]
-    for where in greeted:
-        pl.semaphore_signal(barrier, inc=1, device_id=p.device(**where), device_id_type=MESH)
+    small = [
+        pltpu.make_async_copy(source, target, local_sem.at[6 + k])
+        for k, (source, target) in enumerate(
+            (
+                (decay_hbm, decay_ref),
+                (inmap_hbm, inmap_ref),
+                (param_hbm, param_ref),
+                (gain1_hbm, gain1),
+                (gain2_hbm, gain2),
+                (taps_hbm, taps_ref),
+                (offset_hbm, offsets),
+            )
+        )
+    ]
+    for copy in (weights[0].local, own_stream, *(w.local for w in weights[1:]), *small):
+        copy.start()
     pl.semaphore_wait(barrier, len(greeted))
 
     gather1 = TokenGather(p, 0, held1, 0, ROWS, tsend, trecv)
@@ -356,131 +351,62 @@
     sum2 = [
         TokenSum(p, 1 + 2 * PARTS + c, c, terms2, core2, chip2, near2, last2, tsend, trecv) for c in range(PARTS)
     ]
-    w_in, w_g, w_out, w_u, w_d = weights
-
-    w_in.start()
-    w_g.start()
-    own_stream.wait()
-    gather1.begin()
-    w_out.start()
-    block_diagonal(decay_ref, maps, 0)
-    block_diagonal(inmap_ref, maps, WIDTH)
-    parameter = -param_ref[...]
-    rate = -DECAY_MULTIPLIER * (jnp.maximum(parameter, 0.0) + jnp.log1p(jnp.exp(-jnp.abs(parameter))))
-    w_in.first()
-    w_g.first()
-    gather1.near()
-    w_in.second()
-    w_g.second()
-    w_out.first()
-    w_u.start()
-    gather1.far()
-    w_in.third()
-    w_g.third()
-    w_out.second()
-    gather1.finish()
-
-    @pl.loop(0, PARTS)
-    def _(c):
-        norm_rows(held1, pl.ds(pl.multiple_of(c * PART, PART), PART), gain1_ref, normed)
-
-    w_in.finish()
-    w_g.finish()
-
-    tall = ROWS // 2
-
-    @pl.loop(0, 2)
-    def _(m):
-        rows = pl.ds(pl.multiple_of(m * tall, tall), tall)
+    hidden = w_up.shape[-1]
+    writes = [
+        pltpu.make_async_copy(out_ref.at[pl.ds(c * PART, PART)], out_hbm.at[pl.ds(c * PART, PART)], out_sem.at[c])
+        for c in range(PARTS)
+    ]
+
+    def rows_of(c):
+        return pl.ds(c * PART, PART)
+
+    def prepare():
+        for copy in small:
+            copy.wait()
+        block_diagonal(decay_ref, maps, 0)
+        block_diagonal(inmap_ref, maps, WIDTH)
+        parameter = -param_ref[...]
+        softplus = jnp.maximum(parameter, 0.0) + jnp.log1p(jnp.exp(-jnp.abs(parameter)))
+        rate_ref[...] = -DECAY_MULTIPLIER * softplus
+
+    def begin():
+        own_stream.wait()
+        gather1.begin()
+
+    def columns_of(held, j, depth):
+        pair = held[2 * j : 2 * j + 2].reshape(2, depth, 128)
+        return jnp.concatenate([pair[0], pair[1]], axis=1)
+
+    def inward(m):
+        rows = pl.ds(m * (ROWS // 2), ROWS // 2)
         columns = normed[rows, :]
-        full = w_input[...].reshape(GROUP * WIDTH, WIDTH)
-        values[rows, :] = jnp.dot(columns, full, preferred_element_type=F32).astype(BF16)
-        full = w_gate[...].reshape(GROUP * WIDTH, WIDTH)
-        gates[rows, :] = jnp.dot(columns, full, preferred_element_type=F32).astype(BF16)
-
-    w_out.third()
-    w_u.first()
-    own_offsets.wait()
-    taps = taps_ref[...].astype(F32)
-
-    def columns_of(held, j, depth):
-        pair = held[pl.ds(2 * j, 2)].reshape(2, depth, 128)
-        return jnp.concatenate([pair[0], pair[1]], axis=1)
+        for held, target in ((w_input, values), (w_gate, gates)):
+            full = held[...].reshape(GROUP * WIDTH, WIDTH)
+            target[rows, :] = jnp.dot(columns, full, preferred_element_type=F32).astype(BF16)
 
     def mix(c):
-        rows = pl.ds(c * PART, PART)
-        mixed[rows, :] = mixer_rows(values[rows, :], gates[rows, :], offsets[rows, :], taps, maps[...], rate)
-
-    def project(c, source, held, depth, terms):
-        rows = pl.ds(c * PART, PART)
-
-        @pl.loop(0, GROUP)
-        def _(j):
-            total = jnp.dot(source[rows, :], columns_of(held, j, depth), preferred_element_type=F32)
-            terms[j // 2, lax.rem(j, 2), rows] = total.astype(BF16)
+        rows = rows_of(c)
+        taps = taps_ref[...].astype(F32)
+        mixed[rows, :] = mixer_rows(values[rows, :], gates[rows, :], offsets[rows, :], taps, maps[...], rate_ref[...])
+
+    def project(c, source, held, depth, terms, total):
+        rows = rows_of(c)
+        for j in range(GROUP):
+            product = jnp.dot(source[rows, :], columns_of(held, j, depth), preferred_element_type=F32)
+            terms[j // 2, j % 2, rows] = product.astype(BF16)
+        total.begin()
 
     def middle_of(c):
-        rows = pl.ds(c * PART, PART)
+        rows = rows_of(c)
         held2[p.tp, rows] = sum1[c].finish(held1[p.tp, rows])
         gather2[c].begin()
 
     def raise_rows(c):
-        rows = pl.ds(c * PART, PART)
-        norm_rows(held2, rows, gain2_ref, normed)
-
-    mix(0)
-    w_out.finish()
-    project(0, mixed, w_output, WIDTH, terms1)
-    sum1[0].begin()
-    w_d.start()
-    w_u.second()
-    mix(1)
-    project(1, mixed, w_output, WIDTH, terms1)
-    sum1[1].begin()
-    sum1[0].cores()
-    mix(2)
-    project(2, mixed, w_output, WIDTH, terms1)
-    sum1[2].begin()
-    sum1[1].cores()
-    sum1[0].ring()
-    w_u.third()
-    mix(3)
-    project(3, mixed, w_output, WIDTH, terms1)
-    sum1[3].begin()
-    sum1[2].cores()
-    sum1[1].ring()
-    middle_of(0)
-    w_d.first()
-    sum1[3].cores()
-    sum1[2].ring()
-    middle_of(1)
-    gather2[0].near()
-    sum1[3].ring()
-    middle_of(2)
-    gather2[1].near()
-    gather2[0].far()
-    w_d.second()
-    middle_of(3)
-    gather2[2].near()
-    gather2[1].far()
-    gather2[0].finish()
-    raise_rows(0)
-    gather2[3].near()
-    gather2[2].far()
-    gather2[1].finish()
-    raise_rows(1)
-    gather2[3].far()
-    gather2[2].finish()
-    raise_rows(2)
-    gather2[3].finish()
-    raise_rows(3)
-    w_d.third()
-    w_u.finish()
-
-    hidden = w_up.shape[-1]
+        gather2[c].finish()
+        norm_rows(held2, rows_of(c), gain2, normed)
 
     def lift(c):
-        rows = pl.ds(c * PART, PART)
+        rows = rows_of(c)
         columns = normed[rows, :]
         for n in range(hidden // WIDTH):
             some = slice(n * WIDTH, (n + 1) * WIDTH)
@@ -488,29 +414,52 @@
             raised = jnp.maximum(jnp.dot(columns, full, preferred_element_type=F32), 0.0)
             activity[rows, some] = (raised * raised).astype(BF16)
 
+    def last_of(c):
+        rows = rows_of(c)
+        out_ref[rows, :] = sum2[c].finish(held2[p.tp, rows])
+        writes[c].start()
+
+    actions = {
+        "X": prepare,
+        "GS": begin,
+        "G+": lambda: gather1.near("+"),
+        "G-": lambda: gather1.near("-"),
+        "GB": gather1.far,
+        "GF": gather1.finish,
+        "I0": lambda: inward(0),
+        "I1": lambda: inward(1),
+    }
+    for i, w in enumerate(weights):
+        for name in STEPS:
+            actions[f"{i}{name}"] = functools.partial(w.step, name)
+        actions[f"{i}F"] = w.finish
     for c in range(PARTS):
-        lift(c)
-    w_d.finish()
-
-    def last_of(c):
-        rows = pl.ds(c * PART, PART)
-        out_ref[rows, :] = sum2[c].finish(held2[p.tp, rows])
-
-    for c in range(PARTS + 3):
-        if c < PARTS:
-            project(c, activity, w_down, hidden, terms2)
-            sum2[c].begin()
-        if 0 <= c - 1 < PARTS:
-            sum2[c - 1].cores()
-        if 0 <= c - 2 < PARTS:
-            sum2[c - 2].ring()
-        if 0 <= c - 3 < PARTS:
-            last_of(c - 3)
+        actions[f"N{c}"] = functools.partial(norm_rows, held1, rows_of(c), gain1, normed)
+        actions[f"M{c}"] = functools.partial(mix, c)
+        actions[f"P{c}"] = functools.partial(project, c, mixed, w_output, WIDTH, terms1, sum1[c])
+        actions[f"K{c}"] = sum1[c].cores
+        actions[f"L{c}"] = functools.partial(middle_of, c)
+        actions[f"B{c}"] = gather2[c].far
+        actions[f"Q{c}"] = functools.partial(raise_rows, c)
+        actions[f"U{c}"] = functools.partial(lift, c)
+        actions[f"V{c}"] = functools.partial(project, c, activity, w_down, hidden, terms2, sum2[c])
+        actions[f"k{c}"] = sum2[c].cores
+        actions[f"l{c}"] = functools.partial(last_of, c)
+        for sign in "+-":
+            actions[f"R{c}{sign}"] = functools.partial(sum1[c].ring, sign)
+            actions[f"A{c}{sign}"] = functools.partial(gather2[c].near, sign)
+            actions[f"r{c}{sign}"] = functools.partial(sum2[c].ring, sign)
+    order = " ".join(ORDER).split()
+    assert sorted(order) == sorted(actions)
+    for name in order:
+        actions[name]()
 
     for w in weights:
         w.drain()
     for event in (gather1, *gather2, *sum1, *sum2):
         event.drain()
+    for write in writes:
+        write.wait()
 
 
 def quarters(weight):
@@ -544,7 +493,7 @@
         )
     ]
     hidden = up_projection_weight.shape[1]
-    far, near = pl.BlockSpec(memory_space=pltpu.HBM), pl.BlockSpec(memory_space=pltpu.VMEM)
+    far = pl.BlockSpec(memory_space=pltpu.HBM)
     sums = [
         pltpu.VMEM((4, 2, ROWS, WIDTH), BF16),
         pltpu.VMEM((4, ROWS, WIDTH), BF16),
@@ -556,8 +505,8 @@
     return pl.pallas_call(
         kernel,
         out_shape=jax.ShapeDtypeStruct(stream.shape, stream.dtype),
-        in_specs=[far, near, near, far, far, near, near, near, near, far, far, far, far],
-        out_specs=near,
+        in_specs=[far] * 13,
+        out_specs=far,
         scratch_shapes=[
             *[pltpu.VMEM((16, *w.shape), BF16) for w in cut],
             pltpu.VMEM((GROUP, ROWS, WIDTH), BF16),
@@ -571,7 +520,16 @@
             pltpu.VMEM((WIDTH, 2 * WIDTH), BF16),
             *sums,
             *sums,
-            pltpu.SemaphoreType.DMA((7,)),
+            pltpu.VMEM((1, GROUP * WIDTH), F32),
+            pltpu.VMEM((1, GROUP * WIDTH), F32),
+            pltpu.VMEM(causal_filter_weight.shape, BF16),
+            pltpu.VMEM(decay_gate_matrix.shape, BF16),
+            pltpu.VMEM(input_gate_matrix.shape, BF16),
+            pltpu.VMEM((1, WIDTH), F32),
+            pltpu.VMEM((1, WIDTH), F32),
+            pltpu.VMEM((ROWS, WIDTH), BF16),
+            pltpu.SemaphoreType.DMA((13,)),
+            pltpu.SemaphoreType.DMA((PARTS,)),
             pltpu.SemaphoreType.DMA((5,)),
             pltpu.SemaphoreType.DMA((5, len(KINDS))),
             pltpu.SemaphoreType.DMA((events,)),

time: 93.1 us -> 79 us (0.85)
  the two profiles are of different devices: /device:TPU:4 before, /device:TPU:1 now
where the time goes in v2:
time: 79 us; the launch traced here: 78.8 us
  Pallas kernels  77.2 us (98%)
  local copies, waits for them, and re-layouts  1.67 us (2%)
    pallas_call x1, Pallas kernels, shards(): pl.pallas_call(kernel, out_shape=jax.ShapeDtypeStruct(stream.shape, strea...  77.2 us
    unnamed x1, local copies, waits for them, and re-layouts  1.67 us

profile of v2, /device:TPU:1, one launch (start us, length us, event | category | flops | bytes accessed | tf_op | source)
XLA Modules:
  0.0 78.8 jit_solution(11065939191229500618)
XLA Ops:
  0.0 77.2 %shard_map.127 = bf16[512,256]{1,0:T(8,128)(2,1)} custom-call(bf16[512,256]{1,0:T(8,128)(2,1)} %stream_ref.1, f32[1,2048]{1,0:T(1,128)} %bitcast.13, f32[1,2048]{1,0:T(1,128)} %bitcast.14, bf16[2,2,32,256]{3,2,1,0:T(8,128)(2,1)} %bitcast.10, bf16[2,2,32,256]{3,2,1,0:T(8,128)(2,1)} %bitcast.11, bf16[4,256]{1,0:T(4,128)(2,1)} %taps_hbm.1, ...), custom_call_target="tpu_custom_call" | custom-call | tf_op jit(solution)/shard_map/pallas_call | solution.py:505
  77.2 1.7 %copy.15 = bf16[512,256]{1,0:T(8,128)(2,1)} copy(bf16[512,256]{1,0:T(8,128)(2,1)} %shard_map.127) | data formatting | bytes 524288

commit v3 on v2

v3 whole, which is shorter than its diff:
```python
import functools

import jax
import jax.numpy as jnp
from jax import lax
from jax.experimental import pallas as pl
from jax.experimental.pallas import tpu as pltpu
from jax.sharding import Mesh
from jax.sharding import PartitionSpec as P

MESH = pl.DeviceIdType.MESH
SEQ_LEN = 128
FS = ("fs_0", "fs_1")
REP_FS = ("rep", "fs_0", "fs_1")
AXES = ("rep", "fs_0", "fs_1", "tp")

EPSILON = 1e-06
DECAY_MULTIPLIER = 8.0
F32 = jnp.float32
BF16 = jnp.bfloat16

ROWS, WIDTH, PARTS, GROUP = 512, 256, 4, 8
PART = ROWS // PARTS
HALF = PART // 2
TALL = ROWS // 2
VMEM_LIMIT = 60 * 1024 * 1024
TURNS = (0, -1, 1, 2, 2)

EVERY = slice(None)
STEPS = {
    "S": ((), (("oy+", 0, 0, ()), ("oy-", 0, 0, ()), ("oz+", 0, 0, ()), ("oz-", 0, 0, ()))),
    "a": (
        ("o",),
        (
            ("ry+", 0, -1, (EVERY, 0)), ("rz+", -1, 0, (EVERY, 0)), ("ry-", 0, 1, (EVERY, 1)), ("rz-", 1, 0, (EVERY, 1)),
            ("a1z+", 0, -1, (0,)), ("a1z-", 0, -1, (0,)), ("b1y+", -1, 0, (1,)), ("b1y-", -1, 0, (1,)),
            ("a3z+", 0, 1, (0,)), ("a3z-", 0, 1, (0,)), ("b3y+", 1, 0, (1,)), ("b3y-", 1, 0, (1,)),
        ),
    ),
    "e": (
        ("r",),
        (("a2z+", 0, 2, (0,)), ("a2z-", 0, 2, (0,)), ("b2y+", 2, 0, (1,)), ("b2y-", 2, 0, (1,))),
    ),
    "g": (
        ("1",),
        (("f1z+", -1, -1, (0, 0)), ("f1z-", 1, -1, (0, 1)), ("g1y+", -1, -1, (1, 0)), ("g1y-", -1, 1, (1, 1))),
    ),
    "h": (
        ("3",),
        (("f3z+", -1, 1, (0, 0)), ("f3z-", 1, 1, (0, 1)), ("g3y+", 1, -1, (1, 0)), ("g3y-", 1, 1, (1, 1))),
    ),
    "i": (
        ("2",),
        (("f2z+", -1, 2, (0, 0)), ("f2z-", 1, 2, (0, 1)), ("g2y+", 2, -1, (1, 0)), ("g2y-", 2, 1, (1, 1))),
    ),
}
GROUPS = {
    "o": 16, "r": 8, "1": 8, "3": 8, "2": 8, "down": 2, "up": 2, "beside": 4, "opposite": 4,
}
NAMES = list(GROUPS)


def group_of(name):
    if name[0] in "or":
        return name[0]
    if name[0] in "ab":
        return name[1]
    if name[1] == "2":
        return "opposite"
    return "beside" if name[0] == "f" else {"1": "down", "3": "up"}[name[1]]


def wrap(value, n):
    return lax.rem(value + n, n)


class Place:
    def __init__(self):
        self.rep, self.z, self.y, self.tp = (lax.axis_index(a) for a in AXES)
        self.whole_z = self.rep * 4 + self.z
        self.x, self.core = self.tp // 2, lax.rem(self.tp, 2)
        self.other = 1 - self.core

    def device(self, x=0, y=0, z=0, flip=False):
        z_there = wrap(self.whole_z + z, 8)
        core = self.other if flip else self.core
        return (z_there // 4, lax.rem(z_there, 4), wrap(self.y + y, 4), wrap(self.x + x, 4) * 2 + core)

    def shard(self, z=0, y=0):
        return wrap(self.z + z, 4) * 4 + wrap(self.y + y, 4)

    def slot(self, x=0, flip=False):
        return wrap(self.x + x, 4) * 2 + (self.other if flip else self.core)


class WeightGather:
    def __init__(self, place, index, own_ref, held, local_sem, send_sem, recv_sems):
        self.p, self.i, self.own, self.held = place, index, own_ref, held
        self.local = pltpu.make_async_copy(own_ref, held.at[place.shard()], local_sem.at[index])
        self.send_sem, self.recv_sems = send_sem.at[index], recv_sems

    def go(self, kind, z, y, part):
        where = {"y+": dict(y=1), "y-": dict(y=-1), "z+": dict(z=1), "z-": dict(z=-1)}[kind[-2:]]
        view = self.held.at[(self.p.shard(z, y), *part)]
        copy = pltpu.make_async_remote_copy(
            src_ref=view,
            dst_ref=view,
            send_sem=self.send_sem,
            recv_sem=self.recv_sems.at[self.i, NAMES.index(group_of(kind))],
            device_id=self.p.device(**where),
            device_id_type=MESH,
        )
        copy.start()

    def step(self, name):
        if name == "S":
            self.local.wait()
        waits, sends = STEPS[name]
        self.arrived(*waits)
        for message in sends:
            self.go(*message)

    def arrived(self, *groups):
        for name in groups:
            quarters = GROUPS[name]
            view = self.held.at[pl.ds(0, quarters // 4)] if quarters >= 4 else self.held.at[0, 0]
            pltpu.make_async_copy(view, view, self.recv_sems.at[self.i, NAMES.index(name)]).wait()

    def drain(self):
        view = self.held.at[pl.ds(0, 15)]
        pltpu.make_async_copy(view, view, self.send_sem).wait()


class TokenGather:
    def __init__(self, place, index, held, start, rows, send_sems, recv_sems):
        self.p, self.held, self.start, self.rows = place, held, start, rows
        self.send_sem, self.recv_sems = send_sems.at[index], recv_sems.at[index]
        self.sent = {}

    def go(self, name, sem, slot, device, start=0, rows=None):
        view = self.held.at[slot, pl.ds(self.start + start, rows or self.rows)]
        copy = pltpu.make_async_remote_copy(
            src_ref=view,
            dst_ref=view,
            send_sem=self.send_sem,
            recv_sem=self.recv_sems.at[sem],
            device_id=device,
            device_id_type=MESH,
        )
        copy.start()
        self.sent[name] = copy

    def slots_of(self, slots, sem):
        view = self.held.at[pl.ds(0, slots), pl.ds(self.start, self.rows)]
        pltpu.make_async_copy(view, view, sem).wait()

    def begin(self):
        p = self.p
        self.go("o+", 0, p.slot(), p.device(x=1))
        self.go("o-", 0, p.slot(), p.device(x=-1))
        self.go("p0", 2, p.slot(), p.device(flip=True))

    def near(self):
        p, half = self.p, self.rows // 2
        self.slots_of(2, self.recv_sems.at[0])
        self.go("f+", 1, p.slot(x=-1), p.device(x=1), 0, half)
        self.go("f-", 1, p.slot(x=1), p.device(x=-1), half, half)
        self.go("p1", 2, p.slot(x=-1), p.device(flip=True))
        self.go("p3", 2, p.slot(x=1), p.device(flip=True))

    def far(self):
        p = self.p
        self.slots_of(1, self.recv_sems.at[1])
        self.go("p2", 2, p.slot(x=2), p.device(flip=True))

    def finish(self):
        self.slots_of(4, self.recv_sems.at[2])

    def drain(self):
        self.slots_of(7, self.send_sem)


class TokenSum:
    def __init__(self, place, index, part, terms, from_core, chip, near, last, send_sems, recv_sems):
        self.p, self.part, self.rows = place, part, pl.ds(part * PART, PART)
        self.terms, self.from_core, self.chip, self.near, self.last = terms, from_core, chip, near, last
        self.send_sem, self.recv_sems = send_sems.at[index], recv_sems.at[index]
        self.sent = {}

    def go(self, name, sem, src, dst, device):
        copy = pltpu.make_async_remote_copy(
            src_ref=src,
            dst_ref=dst,
            send_sem=self.send_sem,
            recv_sem=self.recv_sems.at[sem],
            device_id=device,
            device_id_type=MESH,
        )
        copy.start()
        self.sent[name] = copy

    def half(self, h):
        return pl.ds(self.part * PART + h * HALF, HALF)

    def begin(self):
        p = self.p
        self.go("d", 0, self.terms.at[:, p.other, self.rows], self.from_core.at[:, self.rows], p.device(flip=True))

    def chip_sum(self, x):
        p = self.p
        there = wrap(p.x + x, 4)
        return self.terms[there, p.core, self.rows].astype(F32) + self.from_core[there, self.rows].astype(F32)

    def cores(self):
        p, chip = self.p, self.chip
        self.sent["d"].wait_recv()
        right, left, far = wrap(p.x + 1, 4), wrap(p.x - 1, 4), wrap(p.x + 2, 4)
        chip[far, self.rows] = self.chip_sum(2).astype(BF16)
        self.go("h+", 1, chip.at[far, self.half(0)], self.near.at[0, self.half(0)], p.device(x=1))
        self.go("h-", 1, chip.at[far, self.half(1)], self.near.at[1, self.half(1)], p.device(x=-1))
        chip[right, self.rows] = self.chip_sum(1).astype(BF16)
        self.go("e+", 2, chip.at[right, self.half(1)], self.last.at[0, self.half(1)], p.device(x=1))
        chip[left, self.rows] = self.chip_sum(-1).astype(BF16)
        self.go("e-", 2, chip.at[left, self.half(0)], self.last.at[1, self.half(0)], p.device(x=-1))

    def ring(self):
        p = self.p
        both = self.near.at[0, self.rows]
        pltpu.make_async_copy(both, both, self.recv_sems.at[1]).wait()
        for x, side in ((1, 0), (-1, 1)):
            rows = self.half(side)
            total = self.chip[wrap(p.x + x, 4), rows].astype(F32) + self.near[side, rows].astype(F32)
            self.near[side, rows] = total.astype(BF16)
            self.go("e2", 2, self.near.at[side, rows], self.last.at[side, rows], p.device(x=x))

    def finish(self, base):
        both = self.last.at[:, self.rows]
        pltpu.make_async_copy(both, both, self.recv_sems.at[2]).wait()
        total = self.chip_sum(0) + (self.last[0, self.rows].astype(F32) + self.last[1, self.rows].astype(F32))
        return (base.astype(F32) + total).astype(BF16)

    def drain(self):
        view = self.terms.at[:, 0, self.rows]
        part = self.chip.at[pl.ds(0, 3), self.rows]
        pltpu.make_async_copy(view, view, self.send_sem).wait()
        pltpu.make_async_copy(part, part, self.send_sem).wait()


class ColumnSum:
    def __init__(self, place, index, part, terms, from_core, chip, near, last, send_sems, recv_sems):
        self.p, self.start, self.rows = place, part * TALL, pl.ds(part * TALL, TALL)
        self.terms, self.from_core, self.chip, self.near, self.last = terms, from_core, chip, near, last
        self.send_sem, self.recv_sems = send_sems.at[index], recv_sems.at[index]

    def go(self, sem, src, dst, device):
        pltpu.make_async_remote_copy(
            src_ref=src,
            dst_ref=dst,
            send_sem=self.send_sem,
            recv_sem=self.recv_sems.at[sem],
            device_id=device,
            device_id_type=MESH,
        ).start()

    def arrived(self, view, sem):
        pltpu.make_async_copy(view, view, self.recv_sems.at[sem]).wait()

    def half(self, h):
        return pl.ds(self.start + h * (TALL // 2), TALL // 2)

    def chip_sum(self, there, rows):
        return self.terms[there, self.p.core, rows].astype(F32) + self.from_core[there, rows].astype(F32)

    def begin(self, k, core=None):
        there = wrap(self.p.z + k, 4)

        def send():
            terms = self.terms.at[there, self.p.other, self.rows]
            self.go(k, terms, self.from_core.at[there, self.rows], self.p.device(flip=True))

        if core is None:
            send()
        else:
            pl.when(core != self.p.core)(send)

    def away(self, k, core):
        there = wrap(self.p.z + k, 4)
        away = wrap(there - self.p.x, 4)
        return there, away if core is None else jnp.where(core == self.p.core, away, 4)

    def cores(self, k, core=None):
        p, chip = self.p, self.chip
        there, away = self.away(k, core)
        arrived = functools.partial(self.arrived, self.from_core.at[0, self.rows], k)
        if core is None:
            arrived()
        else:
            pl.when(core == p.core)(arrived)

        def add(rows):
            chip[there, rows] = self.chip_sum(there, rows).astype(BF16)

        @pl.when(away == 2)
        def _():
            add(self.rows)
            self.go(4, chip.at[there, self.half(0)], self.near.at[0, self.half(0)], p.device(x=1))
            self.go(5, chip.at[there, self.half(1)], self.near.at[1, self.half(1)], p.device(x=-1))

        for distance, x, side in ((1, 1, 0), (3, -1, 1)):

            @pl.when(away == distance)
            def _(x=x, side=side):
                rows = self.half(1 - side)
                add(rows)
                self.go(6, chip.at[there, rows], self.last.at[side, rows], p.device(x=x))
                add(self.half(side))

    def ring(self, k, core=None):
        p = self.p
        there, away = self.away(k, core)
        for distance, x, side in ((1, 1, 0), (3, -1, 1)):

            @pl.when(away == distance)
            def _(x=x, side=side):
                rows = self.half(side)
                view = self.near.at[side, rows]
                self.arrived(view, 4 + side)
                total = self.chip[there, rows].astype(F32) + self.near[side, rows].astype(F32)
                self.near[side, rows] = total.astype(BF16)
                self.go(6, view, self.last.at[side, rows], p.device(x=x))

    def finish(self, base):
        self.arrived(self.last.at[:, self.rows], 6)
        total = self.chip_sum(self.p.x, self.rows)
        total = total + (self.last[0, self.rows].astype(F32) + self.last[1, self.rows].astype(F32))
        return (base.astype(F32) + total).astype(BF16)

    def drain(self):
        view = self.chip.at[:, self.rows]
        part = self.chip.at[pl.ds(0, 3), self.rows]
        pltpu.make_async_copy(view, view, self.send_sem).wait()
        pltpu.make_async_copy(part, part, self.send_sem).wait()


def norm_rows(held, rows, gain_ref, normed):
    total = jnp.zeros((PART, 1), F32)
    for k in range(GROUP):
        piece = held[k, rows].astype(F32)
        total = total + jnp.sum(piece * piece, axis=-1, keepdims=True)
    inverse = lax.rsqrt(total * (1.0 / (GROUP * WIDTH)) + EPSILON)
    for k in range(GROUP):
        columns = slice(k * WIDTH, (k + 1) * WIDTH)
        piece = held[k, rows].astype(F32) * inverse * gain_ref[:, columns]
        normed[rows, columns] = piece.astype(BF16)


def block_diagonal(matrix_ref, out_ref, offset):
    blocks, size, _ = matrix_ref.shape
    row = lax.broadcasted_iota(jnp.int32, (size, blocks * size), 0)
    column = lax.broadcasted_iota(jnp.int32, (size, blocks * size), 1)
    for b in range(blocks):
        select = (column == row + b * size).astype(F32).astype(BF16)
        spread = jnp.dot(matrix_ref[b], select, preferred_element_type=F32)
        out_ref[b * size : (b + 1) * size, offset : offset + blocks * size] = spread.astype(BF16)


def shifted(values, by, row, fill):
    return jnp.where(row >= by, pltpu.roll(values, by, 0), fill)


def mixer_rows(values, offsets, taps, maps, rate):
    channels = values.shape[1]
    row = lax.broadcasted_iota(jnp.int32, values.shape, 0)
    wide = values.astype(F32)
    reach = taps.shape[0]
    total = taps[0:1] * shifted(wide, reach - 1, row, 0.0)
    for k in range(1, reach):
        by = reach - 1 - k
        total = total + taps[k : k + 1] * (shifted(wide, by, row, 0.0) if by else wide)
    conved = total.astype(BF16)
    both = jax.nn.sigmoid(jnp.dot(conved, maps, preferred_element_type=F32))
    decay = rate * both[:, :channels] + offsets
    factor = jnp.exp(decay)
    twice = 2.0 * decay
    small = -twice * (1.0 + twice * (0.5 + twice * (1.0 / 6.0 + twice * (1.0 / 24.0))))
    lost = jnp.where(twice > -0.03, small, 1.0 - factor * factor)
    state = jnp.sqrt(lost) * both[:, channels:] * conved.astype(F32)
    by = 1
    while by < SEQ_LEN:
        state = factor * shifted(state, by, row, 0.0) + state
        if 2 * by < SEQ_LEN:
            factor = factor * shifted(factor, by, row, 1.0)
        by *= 2
    return state


def gated(state, gates):
    gate = gates.astype(F32)
    gelu = 0.5 * gate * (1.0 + lax.erf(gate * (0.5**0.5)))
    return (state * gelu).astype(BF16)


ORDER = (
    "0S 1S GS X", "2S 0a GA0 1a", "2a 0e GA1 0h", "GB0 GF0 1h 2e", "0g GB1 1e GF1", "0i 3S N0 N3",
    "N2 2g 1g N1", "2h 1i 2i 0F", "4S I0 5S I1", "3a M0 M2 1F", "M3 J1 J0 2F", "P0 M1 4a P1",
    "P2 K0 P3 K1", "5a 3g K2 3e", "K3 4e R0 5g", "R1 5e R2 5h", "4h 3i R3 6S", "4i L0 7S 8S",
    "3h L1 L2 4g", "6a 5i L3 A1", "A0 7a A2 8a", "6e A3 B2 3F", "7e B1 4F 6g", "B0 B3 7g Q1",
    "Q0 8e Q2 8g", "5F U02 6h Q3", "7h U10 U11 U00", "8h 6i U01 U12", "7i V0 8i V1", "V2 k00 V3 V4",
    "k10 k20 k11 k21", "k31 k30 k40 k01", "k41 r10 r00 r20", "r11 r01 r41 r40", "r31 r30 r21 l0", "l1",
)


def kernel(
    stream_ref, gain1_hbm, gain2_hbm, input_ref, gate_ref, taps_hbm, decay_hbm, inmap_hbm, param_hbm, offset_hbm,
    output_ref, up_ref, down_ref,
    out_hbm,
    w_input, w_gate, w_output, w_up0, w_up1, w_up2, w_down0, w_down1, w_down2,
    held1, held2, normed, values, gates, offsets, state, activity, maps,
    terms1, core1, chip1, near1, last1, terms2, core2, chip2, near2, last2,
    gain1, gain2, taps_ref, decay_ref, inmap_ref, param_ref, rate_ref, out_ref,
    local_sem, out_sem, wsend, wrecv, tsend, trecv, csend, crecv,
):
    w_up, w_down = (w_up0, w_up1, w_up2), (w_down0, w_down1, w_down2)
    p = Place()
    barrier = pltpu.get_barrier_semaphore()
    greeted = [dict(x=1), dict(x=-1), dict(y=1), dict(y=-1), dict(z=1), dict(z=-1), dict(flip=True)]
    for where in greeted:
        pl.semaphore_signal(barrier, inc=1, device_id=p.device(**where), device_id_type=MESH)
    blocks = range(len(w_up))
    weights = [
        WeightGather(p, i, own, held, local_sem, wsend, wrecv)
        for i, (own, held) in enumerate(
            (
                (input_ref, w_input),
                (gate_ref, w_gate),
                (output_ref, w_output),
                *((up_ref.at[:, :, :, n * WIDTH : (n + 1) * WIDTH], w_up[n]) for n in blocks),
                *((down_ref.at[n], w_down[n]) for n in blocks),
            )
        )
    ]
    own_stream = pltpu.make_async_copy(stream_ref, held1.at[p.tp], local_sem.at[9])
    small = [
        pltpu.make_async_copy(source, target, local_sem.at[10 + k])
        for k, (source, target) in enumerate(
            (
                (decay_hbm, decay_ref),
                (inmap_hbm, inmap_ref),
                (param_hbm, param_ref),
                (gain1_hbm, gain1),
                (gain2_hbm, gain2),
                (taps_hbm, taps_ref),
                (offset_hbm, offsets),
            )
        )
    ]
    for copy in (weights[0].local, own_stream, *(w.local for w in weights[1:]), *small):
        copy.start()
    pl.semaphore_wait(barrier, len(greeted))

    gather1 = [TokenGather(p, c, held1, c * TALL, TALL, tsend, trecv) for c in range(2)]
    gather2 = [TokenGather(p, 2 + c, held2, c * PART, PART, tsend, trecv) for c in range(PARTS)]
    sum1 = [
        TokenSum(p, 2 + PARTS + c, c, terms1, core1, chip1, near1, last1, tsend, trecv) for c in range(PARTS)
    ]
    sum2 = [ColumnSum(p, c, c, terms2, core2, chip2, near2, last2, csend, crecv) for c in range(2)]
    writes = [
        pltpu.make_async_copy(out_ref.at[pl.ds(c * TALL, TALL)], out_hbm.at[pl.ds(c * TALL, TALL)], out_sem.at[c])
        for c in range(2)
    ]

    def rows_of(c):
        return pl.ds(c * PART, PART)

    def prepare():
        for copy in small:
            copy.wait()
        block_diagonal(decay_ref, maps, 0)
        block_diagonal(inmap_ref, maps, WIDTH)
        parameter = -param_ref[...]
        softplus = jnp.maximum(parameter, 0.0) + jnp.log1p(jnp.exp(-jnp.abs(parameter)))
        rate_ref[...] = -DECAY_MULTIPLIER * softplus

    def begin():
        own_stream.wait()
        for gather in gather1:
            gather.begin()

    def columns_of(held, j, depth):
        pair = held[2 * j : 2 * j + 2].reshape(2, depth, 128)
        return jnp.concatenate([pair[0], pair[1]], axis=1)

    def in_halves(rows, held):
        deep = GROUP * WIDTH // 2
        low, high = (held[8 * h : 8 * h + 8].reshape(deep, WIDTH) for h in range(2))
        low = jnp.dot(normed[rows, :deep], low, preferred_element_type=F32)
        return low + jnp.dot(normed[rows, deep:], high, preferred_element_type=F32)

    def inward(m, held, target):
        rows = pl.ds(m * TALL, TALL)
        target[rows, :] = in_halves(rows, held).astype(BF16)

    def mix(c):
        rows = rows_of(c)
        taps = taps_ref[...].astype(F32)
        state[rows, :] = mixer_rows(values[rows, :], offsets[rows, :], taps, maps[...], rate_ref[...])

    def project(c):
        rows = rows_of(c)
        mixed = gated(state[rows, :], gates[rows, :])
        for j in range(GROUP):
            product = jnp.dot(mixed, columns_of(w_output, j, WIDTH), preferred_element_type=F32)
            terms1[j // 2, j % 2, rows] = product.astype(BF16)
        sum1[c].begin()

    def last_core(turn):
        near = p.y // 2
        return {3: near, 4: 1 - near}.get(turn)

    def lower(turn):
        z, core = TURNS[turn], last_core(turn)
        there = wrap(p.z + z, 4)
        for w in weights[-len(blocks) :]:
            w.arrived(*(() if turn == 0 else (NAMES[turn - 5],)))
        for c in range(2):
            rows = pl.ds(c * TALL, TALL)
            for k in (0, 1) if core is None else (core,):
                product = 0.0
                for n in blocks:
                    pair = w_down[n][pl.ds(there * 4 + 2 * k, 2)].reshape(2, WIDTH, 128)
                    columns = jnp.concatenate([pair[0], pair[1]], axis=1)
                    some = activity[rows, n * WIDTH : (n + 1) * WIDTH]
                    product = product + jnp.dot(some, columns, preferred_element_type=F32)
                terms2[there, k, rows] = product.astype(BF16)
            sum2[c].begin(z % 4, core)

    def middle_of(c):
        rows = rows_of(c)
        held2[p.tp, rows] = sum1[c].finish(held1[p.tp, rows])
        gather2[c].begin()

    def raise_rows(c):
        gather2[c].finish()
        norm_rows(held2, rows_of(c), gain2, normed)

    def lift(c, n):
        rows = pl.ds(c * TALL, TALL)
        raised = jnp.maximum(in_halves(rows, w_up[n]), 0.0)
        activity[rows, n * WIDTH : (n + 1) * WIDTH] = (raised * raised).astype(BF16)

    def last_of(c):
        rows = pl.ds(c * TALL, TALL)
        out_ref[rows, :] = sum2[c].finish(held2[p.tp, rows])
        writes[c].start()

    actions = {
        "X": prepare,
        "GS": begin,
    }
    for i, w in enumerate(weights):
        for name in STEPS:
            actions[f"{i}{name}"] = functools.partial(w.step, name)
        if i < 3 + len(blocks):
            actions[f"{i}F"] = functools.partial(w.arrived, *NAMES[-4:])
    for c in range(PARTS):
        actions[f"N{c}"] = functools.partial(norm_rows, held1, rows_of(c), gain1, normed)
        actions[f"M{c}"] = functools.partial(mix, c)
        actions[f"P{c}"] = functools.partial(project, c)
        actions[f"K{c}"] = sum1[c].cores
        actions[f"L{c}"] = functools.partial(middle_of, c)
        actions[f"B{c}"] = gather2[c].far
        actions[f"Q{c}"] = functools.partial(raise_rows, c)
        actions[f"R{c}"] = sum1[c].ring
        actions[f"A{c}"] = gather2[c].near
    for turn, z in enumerate(TURNS):
        actions[f"V{turn}"] = functools.partial(lower, turn)
        for c in range(2):
            actions[f"k{turn}{c}"] = functools.partial(sum2[c].cores, z % 4, last_core(turn))
            actions[f"r{turn}{c}"] = functools.partial(sum2[c].ring, z % 4, last_core(turn))
    for c in range(2):
        actions[f"GA{c}"] = gather1[c].near
        actions[f"GB{c}"] = gather1[c].far
        actions[f"GF{c}"] = gather1[c].finish
        actions[f"I{c}"] = functools.partial(inward, c, w_input, values)
        actions[f"J{c}"] = functools.partial(inward, c, w_gate, gates)
        for n in blocks:
            actions[f"U{c}{n}"] = functools.partial(lift, c, n)
        actions[f"l{c}"] = functools.partial(last_of, c)
    order = " ".join(ORDER).split()
    assert sorted(order) == sorted(actions)
    for name in order:
        actions[name]()

    for w in weights:
        w.drain()
    for event in (*gather1, *gather2, *sum1, *sum2):
        event.drain()
    for write in writes:
        write.wait()


def quarters(weight):
    rows, columns = weight.shape
    return weight.reshape(2, 2, rows // 4, columns)


def shards(
    stream,
    recurrent_norm_gain,
    feedforward_norm_gain,
    recurrent_input_weight,
    output_gate_weight,
    causal_filter_weight,
    decay_gate_matrix,
    input_gate_matrix,
    channel_decay_param,
    token_decay_offset,
    recurrent_output_weight,
    up_projection_weight,
    down_projection_weight,
):
    mixer = [quarters(w) for w in (recurrent_input_weight, output_gate_weight, recurrent_output_weight)]
    up, hidden = quarters(up_projection_weight), up_projection_weight.shape[1]
    blocks = hidden // WIDTH
    down = down_projection_weight.reshape(blocks, 2, 2, WIDTH // 4, -1)
    far = pl.BlockSpec(memory_space=pltpu.HBM)
    sums = [
        pltpu.VMEM((4, 2, ROWS, WIDTH), BF16),
        pltpu.VMEM((4, ROWS, WIDTH), BF16),
        pltpu.VMEM((4, ROWS, WIDTH), BF16),
        pltpu.VMEM((2, ROWS, WIDTH), BF16),
        pltpu.VMEM((2, ROWS, WIDTH), BF16),
    ]
    events = 2 + 2 * PARTS
    return pl.pallas_call(
        kernel,
        out_shape=jax.ShapeDtypeStruct(stream.shape, stream.dtype),
        in_specs=[far] * 13,
        out_specs=far,
        scratch_shapes=[
            *[pltpu.VMEM((16, *w.shape), BF16) for w in mixer],
            *[pltpu.VMEM((16, *up.shape[:-1], WIDTH), BF16)] * blocks,
            *[pltpu.VMEM((16, *down.shape[1:]), BF16)] * blocks,
            pltpu.VMEM((GROUP, ROWS, WIDTH), BF16),
            pltpu.VMEM((GROUP, ROWS, WIDTH), BF16),
            pltpu.VMEM((ROWS, GROUP * WIDTH), BF16),
            pltpu.VMEM((ROWS, WIDTH), BF16),
            pltpu.VMEM((ROWS, WIDTH), BF16),
            pltpu.VMEM((ROWS, WIDTH), F32),
            pltpu.VMEM((ROWS, WIDTH), F32),
            pltpu.VMEM((ROWS, hidden), BF16),
            pltpu.VMEM((WIDTH, 2 * WIDTH), BF16),
            *sums,
            *sums,
            pltpu.VMEM((1, GROUP * WIDTH), F32),
            pltpu.VMEM((1, GROUP * WIDTH), F32),
            pltpu.VMEM(causal_filter_weight.shape, BF16),
            pltpu.VMEM(decay_gate_matrix.shape, BF16),
            pltpu.VMEM(input_gate_matrix.shape, BF16),
            pltpu.VMEM((1, WIDTH), F32),
            pltpu.VMEM((1, WIDTH), F32),
            pltpu.VMEM((ROWS, WIDTH), BF16),
            pltpu.SemaphoreType.DMA((17,)),
            pltpu.SemaphoreType.DMA((2,)),
            pltpu.SemaphoreType.DMA((3 + 2 * blocks,)),
            pltpu.SemaphoreType.DMA((3 + 2 * blocks, len(GROUPS))),
            pltpu.SemaphoreType.DMA((events,)),
            pltpu.SemaphoreType.DMA((events, 3)),
            pltpu.SemaphoreType.DMA((2,)),
            pltpu.SemaphoreType.DMA((2, 7)),
        ],
        compiler_params=pltpu.CompilerParams(
            collective_id=0, has_side_effects=True, vmem_limit_bytes=VMEM_LIMIT
        ),
    )(
        stream,
        recurrent_norm_gain.reshape(1, -1),
        feedforward_norm_gain.reshape(1, -1),
        mixer[0],
        mixer[1],
        causal_filter_weight,
        decay_gate_matrix,
        input_gate_matrix,
        channel_decay_param.reshape(1, -1),
        token_decay_offset,
        mixer[2],
        up,
        down,
    )


def solution(mesh):
    split = Mesh(
        mesh.devices.reshape(mesh.shape["rep"], 4, 4, mesh.shape["tp"]),
        AXES,
    )
    placed = (
        P(REP_FS, "tp"),
        P(),
        P(),
        P(FS, "tp"),
        P(FS, "tp"),
        P(None, "tp"),
        P("tp", None, None),
        P("tp", None, None),
        P("tp"),
        P(REP_FS, "tp"),
        P("tp", FS),
        P(FS, "tp"),
        P("tp", FS),
    )
    return jax.shard_map(
        shards, mesh=split, in_specs=placed, out_specs=P(REP_FS, "tp"), check_vma=False
    )
```

time: 79 us -> 76.9 us (0.973)
  the two profiles are of different devices: /device:TPU:1 before, /device:TPU:4 now
where the time goes in v3:
time: 76.9 us; the launch traced here: 76.7 us
  Pallas kernels  75.1 us (98%)
  local copies, waits for them, and re-layouts  1.67 us (2%)
    pallas_call x1, Pallas kernels, shards(): pl.pallas_call(kernel, out_shape=jax.ShapeDtypeStruct(stream.shape, strea...  75.1 us
    unnamed x1, local copies, waits for them, and re-layouts  1.67 us

profile of v3, /device:TPU:4, one launch (start us, length us, event | category | flops | bytes accessed | tf_op | source)
XLA Modules:
  0.0 76.7 jit_solution(2968715872953060939)
XLA Ops:
  0.0 75.1 %shard_map.127 = bf16[512,256]{1,0:T(8,128)(2,1)} custom-call(bf16[512,256]{1,0:T(8,128)(2,1)} %stream_ref.1, f32[1,2048]{1,0:T(1,128)} %bitcast.13, f32[1,2048]{1,0:T(1,128)} %bitcast.14, bf16[2,2,32,256]{3,2,1,0:T(8,128)(2,1)} %bitcast.10, bf16[2,2,32,256]{3,2,1,0:T(8,128)(2,1)} %bitcast.11, bf16[4,256]{1,0:T(4,128)(2,1)} %taps_hbm.1, ...), custom_call_target="tpu_custom_call" | custom-call | tf_op jit(solution)/shard_map/pallas_call | solution.py:635
  75.1 1.7 %copy.15 = bf16[512,256]{1,0:T(8,128)(2,1)} copy(bf16[512,256]{1,0:T(8,128)(2,1)} %shard_map.127) | data formatting | bytes 524288

commit v4 on v3

--- a/solution.py
+++ b/solution.py
@@ -30,44 +30,42 @@
 STEPS = {
     "S": ((), (("oy+", 0, 0, ()), ("oy-", 0, 0, ()), ("oz+", 0, 0, ()), ("oz-", 0, 0, ()))),
     "a": (
-        ("o",),
+        ("own",),
         (
-            ("ry+", 0, -1, (EVERY, 0)), ("rz+", -1, 0, (EVERY, 0)), ("ry-", 0, 1, (EVERY, 1)), ("rz-", 1, 0, (EVERY, 1)),
+            ("ry+", 0, -1, (EVERY, 0)), ("ry-", 0, 1, (EVERY, 1)),
             ("a1z+", 0, -1, (0,)), ("a1z-", 0, -1, (0,)), ("b1y+", -1, 0, (1,)), ("b1y-", -1, 0, (1,)),
             ("a3z+", 0, 1, (0,)), ("a3z-", 0, 1, (0,)), ("b3y+", 1, 0, (1,)), ("b3y-", 1, 0, (1,)),
         ),
     ),
-    "e": (
-        ("r",),
-        (("a2z+", 0, 2, (0,)), ("a2z-", 0, 2, (0,)), ("b2y+", 2, 0, (1,)), ("b2y-", 2, 0, (1,))),
-    ),
+    "b": ((), (("rz+", -1, 0, (EVERY, 0)), ("rz-", 1, 0, (EVERY, 1)))),
+    "e": (("ry",), (("a2z+", 0, 2, (0,)), ("a2z-", 0, 2, (0,)))),
+    "f": (("rz",), (("b2y+", 2, 0, (1,)), ("b2y-", 2, 0, (1,)))),
     "g": (
-        ("1",),
-        (("f1z+", -1, -1, (0, 0)), ("f1z-", 1, -1, (0, 1)), ("g1y+", -1, -1, (1, 0)), ("g1y-", -1, 1, (1, 1))),
+        ("by",),
+        (("g1y+", -1, -1, (1, 0)), ("g1y-", -1, 1, (1, 1)), ("g3y+", 1, -1, (1, 0)), ("g3y-", 1, 1, (1, 1))),
     ),
     "h": (
-        ("3",),
-        (("f3z+", -1, 1, (0, 0)), ("f3z-", 1, 1, (0, 1)), ("g3y+", 1, -1, (1, 0)), ("g3y-", 1, 1, (1, 1))),
+        ("az",),
+        (("f1z+", -1, -1, (0, 0)), ("f1z-", 1, -1, (0, 1)), ("f3z+", -1, 1, (0, 0)), ("f3z-", 1, 1, (0, 1))),
     ),
-    "i": (
-        ("2",),
-        (("f2z+", -1, 2, (0, 0)), ("f2z-", 1, 2, (0, 1)), ("g2y+", 2, -1, (1, 0)), ("g2y-", 2, 1, (1, 1))),
-    ),
+    "i": (("a2",), (("f2z+", -1, 2, (0, 0)), ("f2z-", 1, 2, (0, 1)))),
+    "j": (("b2",), (("g2y+", 2, -1, (1, 0)), ("g2y-", 2, 1, (1, 1)))),
 }
 GROUPS = {
-    "o": 16, "r": 8, "1": 8, "3": 8, "2": 8, "down": 2, "up": 2, "beside": 4, "opposite": 4,
+    "own": 16, "ry": 4, "rz": 4, "by": 8, "az": 8, "a2": 4, "b2": 4, "below": 2, "above": 2, "beside": 4, "opposite": 4,
 }
 NAMES = list(GROUPS)
 
 
 def group_of(name):
-    if name[0] in "or":
-        return name[0]
-    if name[0] in "ab":
-        return name[1]
-    if name[1] == "2":
+    way, step, link = name[0], name[1], name[-2]
+    if way in "or":
+        return {"o": "own", "r": "r" + link}[way]
+    if way in "ab":
+        return way + ("2" if step == "2" else link)
+    if step == "2":
         return "opposite"
-    return "beside" if name[0] == "f" else {"1": "down", "3": "up"}[name[1]]
+    return "beside" if way == "f" else {"1": "below", "3": "above"}[step]
 
 
 def wrap(value, n):
@@ -401,12 +399,13 @@
 
 
 ORDER = (
-    "0S 1S GS X", "2S 0a GA0 1a", "2a 0e GA1 0h", "GB0 GF0 1h 2e", "0g GB1 1e GF1", "0i 3S N0 N3",
-    "N2 2g 1g N1", "2h 1i 2i 0F", "4S I0 5S I1", "3a M0 M2 1F", "M3 J1 J0 2F", "P0 M1 4a P1",
-    "P2 K0 P3 K1", "5a 3g K2 3e", "K3 4e R0 5g", "R1 5e R2 5h", "4h 3i R3 6S", "4i L0 7S 8S",
-    "3h L1 L2 4g", "6a 5i L3 A1", "A0 7a A2 8a", "6e A3 B2 3F", "7e B1 4F 6g", "B0 B3 7g Q1",
-    "Q0 8e Q2 8g", "5F U02 6h Q3", "7h U10 U11 U00", "8h 6i U01 U12", "7i V0 8i V1", "V2 k00 V3 V4",
-    "k10 k20 k11 k21", "k31 k30 k40 k01", "k41 r10 r00 r20", "r11 r01 r41 r40", "r31 r30 r21 l0", "l1",
+    "0S 1S 2S GS", "X 0a 1a 0b", "1b 2a 2b GA0", "0e 0f GB0 GA1", "1e 1f 0g 2e", "1g 1h 2f 0h",
+    "0i GF0 0j N1", "GB1 1j 1i 2h", "3S N0 2g GF1", "2i N2 2j N3", "0F 4S 1F 5S", "I1 I0 M0 M3",
+    "3a 2F P0 P3", "M2 3b M1 6S", "4a P2 K0 P1", "K2 K1 K3 5a", "3e 4b 5b 6a", "R0 R1 R2 7S",
+    "3h R3 8S L0", "5f 5g L1 5e", "5h 4f L3 4h", "6b 3f L2 4g", "4e 3i 5j 7a", "A0 7b 3g A1",
+    "5i 3j 4j A3", "A2 4i 8a B0", "B1 6g Q0 7e", "Q1 3F 5F B3", "6f 8b 7g B2", "6e 4F U0 8e",
+    "7h Q2 Q3 6h", "8h 8g 7f U1", "8f V0 8i 6i", "6j 7i V1 V2", "7j k01 8j V3", "k00 k10 k11 k21",
+    "V4 k30 k20 r10", "k40 k41 k31 r21", "r00 r30 r01 r20", "r11 r40 r31 r41", "l0 l1",
 )
 
 
@@ -490,15 +489,12 @@
         pair = held[2 * j : 2 * j + 2].reshape(2, depth, 128)
         return jnp.concatenate([pair[0], pair[1]], axis=1)
 
-    def in_halves(rows, held):
-        deep = GROUP * WIDTH // 2
-        low, high = (held[8 * h : 8 * h + 8].reshape(deep, WIDTH) for h in range(2))
-        low = jnp.dot(normed[rows, :deep], low, preferred_element_type=F32)
-        return low + jnp.dot(normed[rows, deep:], high, preferred_element_type=F32)
-
-    def inward(m, held, target):
+    def inward(m):
         rows = pl.ds(m * TALL, TALL)
-        target[rows, :] = in_halves(rows, held).astype(BF16)
+        columns = normed[rows, :]
+        for held, target in ((w_input, values), (w_gate, gates)):
+            full = held[...].reshape(GROUP * WIDTH, WIDTH)
+            target[rows, :] = jnp.dot(columns, full, preferred_element_type=F32).astype(BF16)
 
     def mix(c):
         rows = rows_of(c)
@@ -543,10 +539,13 @@
         gather2[c].finish()
         norm_rows(held2, rows_of(c), gain2, normed)
 
-    def lift(c, n):
+    def lift(c):
         rows = pl.ds(c * TALL, TALL)
-        raised = jnp.maximum(in_halves(rows, w_up[n]), 0.0)
-        activity[rows, n * WIDTH : (n + 1) * WIDTH] = (raised * raised).astype(BF16)
+        columns = normed[rows, :]
+        for n in blocks:
+            full = w_up[n][...].reshape(GROUP * WIDTH, WIDTH)
+            raised = jnp.maximum(jnp.dot(columns, full, preferred_element_type=F32), 0.0)
+            activity[rows, n * WIDTH : (n + 1) * WIDTH] = (raised * raised).astype(BF16)
 
     def last_of(c):
         rows = pl.ds(c * TALL, TALL)
@@ -581,10 +580,8 @@
         actions[f"GA{c}"] = gather1[c].near
         actions[f"GB{c}"] = gather1[c].far
         actions[f"GF{c}"] = gather1[c].finish
-        actions[f"I{c}"] = functools.partial(inward, c, w_input, values)
-        actions[f"J{c}"] = functools.partial(inward, c, w_gate, gates)
-        for n in blocks:
-            actions[f"U{c}{n}"] = functools.partial(lift, c, n)
+        actions[f"I{c}"] = functools.partial(inward, c)
+        actions[f"U{c}"] = functools.partial(lift, c)
         actions[f"l{c}"] = functools.partial(last_of, c)
     order = " ".join(ORDER).split()
     assert sorted(order) == sorted(actions)

time: 76.9 us -> 77.2 us (level)
  no operation moved by 1% of the time
where the time goes in v4:
time: 77.2 us; the launch traced here: 77.1 us
  Pallas kernels  75.4 us (98%)
  local copies, waits for them, and re-layouts  1.67 us (2%)
    pallas_call x1, Pallas kernels, shards(): pl.pallas_call(kernel, out_shape=jax.ShapeDtypeStruct(stream.shape, strea...  75.4 us
    unnamed x1, local copies, waits for them, and re-layouts  1.67 us

profile of v4, /device:TPU:4, one launch (start us, length us, event | category | flops | bytes accessed | tf_op | source)
XLA Modules:
  0.0 77.1 jit_solution(7313391882467018524)
XLA Ops:
  0.0 75.4 %shard_map.127 = bf16[512,256]{1,0:T(8,128)(2,1)} custom-call(bf16[512,256]{1,0:T(8,128)(2,1)} %stream_ref.1, f32[1,2048]{1,0:T(1,128)} %bitcast.13, f32[1,2048]{1,0:T(1,128)} %bitcast.14, bf16[2,2,32,256]{3,2,1,0:T(8,128)(2,1)} %bitcast.10, bf16[2,2,32,256]{3,2,1,0:T(8,128)(2,1)} %bitcast.11, bf16[4,256]{1,0:T(4,128)(2,1)} %taps_hbm.1, ...), custom_call_target="tpu_custom_call" | custom-call | tf_op jit(solution)/shard_map/pallas_call | solution.py:632
  75.4 1.7 %copy.15 = bf16[512,256]{1,0:T(8,128)(2,1)} copy(bf16[512,256]{1,0:T(8,128)(2,1)} %shard_map.127) | data formatting | bytes 524288

commit v5 on v4

--- a/solution.py
+++ b/solution.py
@@ -23,7 +23,7 @@
 PART = ROWS // PARTS
 HALF = PART // 2
 TALL = ROWS // 2
-VMEM_LIMIT = 60 * 1024 * 1024
+VMEM_LIMIT = 40 * 1024 * 1024
 TURNS = (0, -1, 1, 2, 2)
 
 EVERY = slice(None)
@@ -55,6 +55,7 @@
     "own": 16, "ry": 4, "rz": 4, "by": 8, "az": 8, "a2": 4, "b2": 4, "below": 2, "above": 2, "beside": 4, "opposite": 4,
 }
 NAMES = list(GROUPS)
+TOGETHER = len(NAMES) - 3
 
 
 def group_of(name):
@@ -92,10 +93,10 @@
 
 
 class WeightGather:
-    def __init__(self, place, index, own_ref, held, local_sem, send_sem, recv_sems):
+    def __init__(self, place, index, own_ref, held, local_sem, send_sem, recv_sems, apart):
         self.p, self.i, self.own, self.held = place, index, own_ref, held
         self.local = pltpu.make_async_copy(own_ref, held.at[place.shard()], local_sem.at[index])
-        self.send_sem, self.recv_sems = send_sem.at[index], recv_sems
+        self.send_sem, self.recv_sems, self.apart = send_sem.at[index], recv_sems, apart
 
     def go(self, kind, z, y, part):
         where = {"y+": dict(y=1), "y-": dict(y=-1), "z+": dict(z=1), "z-": dict(z=-1)}[kind[-2:]]
@@ -104,7 +105,7 @@
             src_ref=view,
             dst_ref=view,
             send_sem=self.send_sem,
-            recv_sem=self.recv_sems.at[self.i, NAMES.index(group_of(kind))],
+            recv_sem=self.semaphore(group_of(kind)),
             device_id=self.p.device(**where),
             device_id_type=MESH,
         )
@@ -118,11 +119,21 @@
         for message in sends:
             self.go(*message)
 
+    def semaphore(self, name):
+        k = NAMES.index(name)
+        if self.apart < 0:
+            return self.recv_sems.at[self.i * TOGETHER + min(k, TOGETHER - 1)]
+        return self.recv_sems.at[self.i * TOGETHER + self.apart * (len(NAMES) - TOGETHER) + k]
+
+    def finish(self):
+        view = self.held.at[pl.ds(0, 3)]
+        pltpu.make_async_copy(view, view, self.semaphore(NAMES[-1])).wait()
+
     def arrived(self, *groups):
         for name in groups:
             quarters = GROUPS[name]
             view = self.held.at[pl.ds(0, quarters // 4)] if quarters >= 4 else self.held.at[0, 0]
-            pltpu.make_async_copy(view, view, self.recv_sems.at[self.i, NAMES.index(name)]).wait()
+            pltpu.make_async_copy(view, view, self.semaphore(name)).wait()
 
     def drain(self):
         view = self.held.at[pl.ds(0, 15)]
@@ -412,12 +423,12 @@
 def kernel(
     stream_ref, gain1_hbm, gain2_hbm, input_ref, gate_ref, taps_hbm, decay_hbm, inmap_hbm, param_hbm, offset_hbm,
     output_ref, up_ref, down_ref,
-    out_hbm,
+    out_ref,
     w_input, w_gate, w_output, w_up0, w_up1, w_up2, w_down0, w_down1, w_down2,
     held1, held2, normed, values, gates, offsets, state, activity, maps,
     terms1, core1, chip1, near1, last1, terms2, core2, chip2, near2, last2,
-    gain1, gain2, taps_ref, decay_ref, inmap_ref, param_ref, rate_ref, out_ref,
-    local_sem, out_sem, wsend, wrecv, tsend, trecv, csend, crecv,
+    gain1, gain2, taps_ref, decay_ref, inmap_ref, param_ref, rate_ref,
+    local_sem, wsend, wrecv, tsend, trecv, csend, crecv,
 ):
     w_up, w_down = (w_up0, w_up1, w_up2), (w_down0, w_down1, w_down2)
     p = Place()
@@ -427,7 +438,7 @@
         pl.semaphore_signal(barrier, inc=1, device_id=p.device(**where), device_id_type=MESH)
     blocks = range(len(w_up))
     weights = [
-        WeightGather(p, i, own, held, local_sem, wsend, wrecv)
+        WeightGather(p, i, own, held, local_sem, wsend, wrecv, i - 3 - len(blocks))
         for i, (own, held) in enumerate(
             (
                 (input_ref, w_input),
@@ -463,11 +474,6 @@
         TokenSum(p, 2 + PARTS + c, c, terms1, core1, chip1, near1, last1, tsend, trecv) for c in range(PARTS)
     ]
     sum2 = [ColumnSum(p, c, c, terms2, core2, chip2, near2, last2, csend, crecv) for c in range(2)]
-    writes = [
-        pltpu.make_async_copy(out_ref.at[pl.ds(c * TALL, TALL)], out_hbm.at[pl.ds(c * TALL, TALL)], out_sem.at[c])
-        for c in range(2)
-    ]
-
     def rows_of(c):
         return pl.ds(c * PART, PART)
 
@@ -550,7 +556,6 @@
     def last_of(c):
         rows = pl.ds(c * TALL, TALL)
         out_ref[rows, :] = sum2[c].finish(held2[p.tp, rows])
-        writes[c].start()
 
     actions = {
         "X": prepare,
@@ -560,7 +565,7 @@
         for name in STEPS:
             actions[f"{i}{name}"] = functools.partial(w.step, name)
         if i < 3 + len(blocks):
-            actions[f"{i}F"] = functools.partial(w.arrived, *NAMES[-4:])
+            actions[f"{i}F"] = w.finish
     for c in range(PARTS):
         actions[f"N{c}"] = functools.partial(norm_rows, held1, rows_of(c), gain1, normed)
         actions[f"M{c}"] = functools.partial(mix, c)
@@ -592,8 +597,6 @@
         w.drain()
     for event in (*gather1, *gather2, *sum1, *sum2):
         event.drain()
-    for write in writes:
-        write.wait()
 
 
 def quarters(weight):
@@ -620,6 +623,21 @@
     up, hidden = quarters(up_projection_weight), up_projection_weight.shape[1]
     blocks = hidden // WIDTH
     down = down_projection_weight.reshape(blocks, 2, 2, WIDTH // 4, -1)
+    arguments = (
+        stream,
+        recurrent_norm_gain.reshape(1, -1),
+        feedforward_norm_gain.reshape(1, -1),
+        mixer[0],
+        mixer[1],
+        causal_filter_weight,
+        decay_gate_matrix,
+        input_gate_matrix,
+        channel_decay_param.reshape(1, -1),
+        token_decay_offset,
+        mixer[2],
+        up,
+        down,
+    )
     far = pl.BlockSpec(memory_space=pltpu.HBM)
     sums = [
         pltpu.VMEM((4, 2, ROWS, WIDTH), BF16),
@@ -633,7 +651,7 @@
         kernel,
         out_shape=jax.ShapeDtypeStruct(stream.shape, stream.dtype),
         in_specs=[far] * 13,
-        out_specs=far,
+        out_specs=pl.BlockSpec(memory_space=pltpu.VMEM),
         scratch_shapes=[
             *[pltpu.VMEM((16, *w.shape), BF16) for w in mixer],
             *[pltpu.VMEM((16, *up.shape[:-1], WIDTH), BF16)] * blocks,
@@ -656,11 +674,9 @@
             pltpu.VMEM(input_gate_matrix.shape, BF16),
             pltpu.VMEM((1, WIDTH), F32),
             pltpu.VMEM((1, WIDTH), F32),
-            pltpu.VMEM((ROWS, WIDTH), BF16),
             pltpu.SemaphoreType.DMA((17,)),
-            pltpu.SemaphoreType.DMA((2,)),
             pltpu.SemaphoreType.DMA((3 + 2 * blocks,)),
-            pltpu.SemaphoreType.DMA((3 + 2 * blocks, len(GROUPS))),
+            pltpu.SemaphoreType.DMA(((3 + 2 * blocks) * TOGETHER + blocks * (len(NAMES) - TOGETHER),)),
             pltpu.SemaphoreType.DMA((events,)),
             pltpu.SemaphoreType.DMA((events, 3)),
             pltpu.SemaphoreType.DMA((2,)),
@@ -669,21 +685,7 @@
         compiler_params=pltpu.CompilerParams(
             collective_id=0, has_side_effects=True, vmem_limit_bytes=VMEM_LIMIT
         ),
-    )(
-        stream,
-        recurrent_norm_gain.reshape(1, -1),
-        feedforward_norm_gain.reshape(1, -1),
-        mixer[0],
-        mixer[1],
-        causal_filter_weight,
-        decay_gate_matrix,
-        input_gate_matrix,
-        channel_decay_param.reshape(1, -1),
-        token_decay_offset,
-        mixer[2],
-        up,
-        down,
-    )
+    )(*(pltpu.with_memory_space_constraint(value, pltpu.HBM) for value in arguments))
 
 
 def solution(mesh):

time: 77.2 us -> 75.4 us (0.977)
  local copies, waits for them, and re-layouts: 1.67 us -> 0.71 us
  Pallas kernels: 75.4 us -> 74.6 us
    unnamed x1, local copies, waits for them, and re-layouts: 1.67 us -> 0.71 us
    pallas_call x1, Pallas kernels: 75.4 us -> 74.6 us  [shards(): pl.pallas_call(kernel, out_shape=jax.ShapeDtypeStruct(stream.shape, strea...]
where the time goes in v5:
time: 75.4 us; the launch traced here: 75.3 us
  Pallas kernels  74.6 us (99%)
    pallas_call x1, Pallas kernels, shards(): pl.pallas_call(kernel, out_shape=jax.ShapeDtypeStruct(stream.shape, strea...  74.6 us

profile of v5, /device:TPU:4, one launch (start us, length us, event | category | flops | bytes accessed | tf_op | source)
XLA Modules:
  0.0 75.3 jit_solution(17446393497758244044)
XLA Ops:
  0.0 74.6 %shard_map.127 = bf16[512,256]{1,0:T(8,128)(2,1)S(1)} custom-call(bf16[512,256]{1,0:T(8,128)(2,1)} %stream_ref.1, f32[1,2048]{1,0:T(1,128)} %bitcast.13, f32[1,2048]{1,0:T(1,128)} %bitcast.14, bf16[2,2,32,256]{3,2,1,0:T(8,128)(2,1)} %bitcast.10, bf16[2,2,32,256]{3,2,1,0:T(8,128)(2,1)} %bitcast.11, bf16[4,256]{1,0:T(4,128)(2,1)} %taps_hbm.1, ...), custom_call_target="tpu_custom_call" | custom-call | tf_op jit(solution)/shard_map/pallas_call | solution.py:650
  74.6 0.7 copy.15

commit v6 on v5

--- a/solution.py
+++ b/solution.py
@@ -410,13 +410,13 @@
 
 
 ORDER = (
-    "0S 1S 2S GS", "X 0a 1a 0b", "1b 2a 2b GA0", "0e 0f GB0 GA1", "1e 1f 0g 2e", "1g 1h 2f 0h",
-    "0i GF0 0j N1", "GB1 1j 1i 2h", "3S N0 2g GF1", "2i N2 2j N3", "0F 4S 1F 5S", "I1 I0 M0 M3",
-    "3a 2F P0 P3", "M2 3b M1 6S", "4a P2 K0 P1", "K2 K1 K3 5a", "3e 4b 5b 6a", "R0 R1 R2 7S",
-    "3h R3 8S L0", "5f 5g L1 5e", "5h 4f L3 4h", "6b 3f L2 4g", "4e 3i 5j 7a", "A0 7b 3g A1",
-    "5i 3j 4j A3", "A2 4i 8a B0", "B1 6g Q0 7e", "Q1 3F 5F B3", "6f 8b 7g B2", "6e 4F U0 8e",
-    "7h Q2 Q3 6h", "8h 8g 7f U1", "8f V0 8i 6i", "6j 7i V1 V2", "7j k01 8j V3", "k00 k10 k11 k21",
-    "V4 k30 k20 r10", "k40 k41 k31 r21", "r00 r30 r01 r20", "r11 r40 r31 r41", "l0 l1",
+    "0S GS 1S 2S", "0a GA0 0b 1a", "1b GA1 2a 2b", "0f X 1e 0e", "GB0 1f 0g 0h", "1h GB1 1g 2e",
+    "2h 2f 2g 1j", "GF1 1i GF0 0i", "0j 3S N0 N3", "2i 2j N1 4S", "5S 7S N2 0F", "1F I1 I0 M0",
+    "2F P0 M2 P2", "8S M1 P1 6S", "M3 K0 P3 3a", "K2 K1 4a 4b", "5a R0 K3 R1", "3b 3e R2 5b",
+    "7a R3 L0 6a", "5e L1 4g 4f", "6b L2 7b 5f", "4e L3 8a A0", "3f 5i 6h A1", "8b 3h A2 3g",
+    "5h 5j 4h 4j", "4i A3 3i 6e", "7e 7h 5g 8e", "7f 3j B1 B0", "B2 8h 6g B3", "8g 6f Q0 7g",
+    "Q2 5F 8f Q1", "4F Q3 3F U0", "U1 7j 6j 6i", "V0 8i 7i V1", "8j V2 V3 k00", "k01 k10 k20 V4",
+    "k11 k30 k31 k21", "k40 k41 r10 r00", "r20 r30 r11 r01", "r40 r21 r31 r41", "l0 l1",
 )
 
 

time: 75.4 us -> 74.3 us (0.985)
  Pallas kernels: 74.6 us -> 73.5 us
    pallas_call x1, Pallas kernels: 74.6 us -> 73.5 us  [shards(): pl.pallas_call(kernel, out_shape=jax.ShapeDtypeStruct(stream.shape, strea...]
where the time goes in v6:
time: 74.3 us
  Pallas kernels  73.5 us (99%)
    pallas_call x1, Pallas kernels, shards(): pl.pallas_call(kernel, out_shape=jax.ShapeDtypeStruct(stream.shape, strea...  73.5 us

profile of v6, /device:TPU:4, one launch (start us, length us, event | category | flops | bytes accessed | tf_op | source)
XLA Modules:
  0.0 74.3 jit_solution(13761348667268272315)
XLA Ops:
  0.0 73.5 %shard_map.127 = bf16[512,256]{1,0:T(8,128)(2,1)S(1)} custom-call(bf16[512,256]{1,0:T(8,128)(2,1)} %stream_ref.1, f32[1,2048]{1,0:T(1,128)} %bitcast.13, f32[1,2048]{1,0:T(1,128)} %bitcast.14, bf16[2,2,32,256]{3,2,1,0:T(8,128)(2,1)} %bitcast.10, bf16[2,2,32,256]{3,2,1,0:T(8,128)(2,1)} %bitcast.11, bf16[4,256]{1,0:T(4,128)(2,1)} %taps_hbm.1, ...), custom_call_target="tpu_custom_call" | custom-call | tf_op jit(solution)/shard_map/pallas_call | solution.py:650
  73.6 0.7 copy.15

commit v7 on v6

--- a/solution.py
+++ b/solution.py
@@ -410,13 +410,13 @@
 
 
 ORDER = (
-    "0S GS 1S 2S", "0a GA0 0b 1a", "1b GA1 2a 2b", "0f X 1e 0e", "GB0 1f 0g 0h", "1h GB1 1g 2e",
-    "2h 2f 2g 1j", "GF1 1i GF0 0i", "0j 3S N0 N3", "2i 2j N1 4S", "5S 7S N2 0F", "1F I1 I0 M0",
-    "2F P0 M2 P2", "8S M1 P1 6S", "M3 K0 P3 3a", "K2 K1 4a 4b", "5a R0 K3 R1", "3b 3e R2 5b",
-    "7a R3 L0 6a", "5e L1 4g 4f", "6b L2 7b 5f", "4e L3 8a A0", "3f 5i 6h A1", "8b 3h A2 3g",
-    "5h 5j 4h 4j", "4i A3 3i 6e", "7e 7h 5g 8e", "7f 3j B1 B0", "B2 8h 6g B3", "8g 6f Q0 7g",
-    "Q2 5F 8f Q1", "4F Q3 3F U0", "U1 7j 6j 6i", "V0 8i 7i V1", "8j V2 V3 k00", "k01 k10 k20 V4",
-    "k11 k30 k31 k21", "k40 k41 r10 r00", "r20 r30 r11 r01", "r40 r21 r31 r41", "l0 l1",
+    "0S GS 1S 2S", "0a 0b 1a GA0", "1b 2a GA1 0f", "2b 1e 0e 1h", "1f X GB0 0g", "1g 2e 0h 2f",
+    "2g 1i 2h GF0", "GB1 1j 0j 0i", "3S N1 GF1 2i", "N3 2j 4S 5S", "N2 N0 1F 0F", "I1 7S I0 M0",
+    "2F 3a P0 M2", "6S P2 M1 4a", "M3 3b K0 P1", "P3 5a K2 K1", "R0 4b 8S K3", "5b 4e 7a R1",
+    "R2 7b L0 4f", "5e 6a 6b 3f", "R3 L1 5f 8a", "3e L2 8b 5h", "L3 5g 4h 7f", "5i A0 6e 3g",
+    "4j A1 4i A2", "3j 4g 3h 5j", "A3 6f 8f 3i", "B0 7e 8h B1", "B2 6h 8e Q0", "6g 8g 7g 7h",
+    "6i B3 Q1 7j", "Q2 5F 4F 3F", "U0 Q3 U1 V0", "8j 8i 7i 6j", "V1 V2 V3 k00", "k10 k20 k31 V4",
+    "k21 k11 k01 k30", "k40 r00 k41 r20", "r10 r01 r30 r11", "r21 r40 r31 r41", "l0 l1",
 )
 
 

time: 74.3 us -> 73.3 us (0.987)
  Pallas kernels: 73.5 us -> 72.5 us
    pallas_call x1, Pallas kernels: 73.5 us -> 72.5 us  [shards(): pl.pallas_call(kernel, out_shape=jax.ShapeDtypeStruct(stream.shape, strea...]
where the time goes in v7:
time: 73.3 us; the launch traced here: 73.2 us
  Pallas kernels  72.5 us (99%)
    pallas_call x1, Pallas kernels, shards(): pl.pallas_call(kernel, out_shape=jax.ShapeDtypeStruct(stream.shape, strea...  72.5 us

profile of v7, /device:TPU:4, one launch (start us, length us, event | category | flops | bytes accessed | tf_op | source)
XLA Modules:
  0.0 73.2 jit_solution(16578763263205355839)
XLA Ops:
  0.0 72.5 %shard_map.127 = bf16[512,256]{1,0:T(8,128)(2,1)S(1)} custom-call(bf16[512,256]{1,0:T(8,128)(2,1)} %stream_ref.1, f32[1,2048]{1,0:T(1,128)} %bitcast.13, f32[1,2048]{1,0:T(1,128)} %bitcast.14, bf16[2,2,32,256]{3,2,1,0:T(8,128)(2,1)} %bitcast.10, bf16[2,2,32,256]{3,2,1,0:T(8,128)(2,1)} %bitcast.11, bf16[4,256]{1,0:T(4,128)(2,1)} %taps_hbm.1, ...), custom_call_target="tpu_custom_call" | custom-call | tf_op jit(solution)/shard_map/pallas_call | solution.py:650
  72.5 0.7 copy.15

commit v8 on v7

--- a/solution.py
+++ b/solution.py
@@ -410,13 +410,13 @@
 
 
 ORDER = (
-    "0S GS 1S 2S", "0a 0b 1a GA0", "1b 2a GA1 0f", "2b 1e 0e 1h", "1f X GB0 0g", "1g 2e 0h 2f",
-    "2g 1i 2h GF0", "GB1 1j 0j 0i", "3S N1 GF1 2i", "N3 2j 4S 5S", "N2 N0 1F 0F", "I1 7S I0 M0",
-    "2F 3a P0 M2", "6S P2 M1 4a", "M3 3b K0 P1", "P3 5a K2 K1", "R0 4b 8S K3", "5b 4e 7a R1",
-    "R2 7b L0 4f", "5e 6a 6b 3f", "R3 L1 5f 8a", "3e L2 8b 5h", "L3 5g 4h 7f", "5i A0 6e 3g",
-    "4j A1 4i A2", "3j 4g 3h 5j", "A3 6f 8f 3i", "B0 7e 8h B1", "B2 6h 8e Q0", "6g 8g 7g 7h",
-    "6i B3 Q1 7j", "Q2 5F 4F 3F", "U0 Q3 U1 V0", "8j 8i 7i 6j", "V1 V2 V3 k00", "k10 k20 k31 V4",
-    "k21 k11 k01 k30", "k40 r00 k41 r20", "r10 r01 r30 r11", "r21 r40 r31 r41", "l0 l1",
+    "0S GS 1S 2S", "0a X 0b GA0", "1a 1b 2a 0e", "2b GA1 1e 0f", "0h 0g 1f GB0", "2e GB1 1g 6S",
+    "1h 0i 2f GF1", "GF0 0j N2 1i", "1j 2g 3S 2i", "2h N3 N0 2j", "4S N1 5S 1F", "7S 0F I1 I0",
+    "M0 M2 2F P0", "M1 P1 3a M3", "P2 3b 4a K0", "K1 8S P3 K2", "5a R0 4b K3", "3f 5b 3e 7a",
+    "4e R1 6a R2", "R3 L0 5e 8a", "5f L1 L2 6b", "4f L3 4g 5h", "3i 7b 4h 7g", "3g A1 3h 8b",
+    "A0 4i A2 5g", "A3 4j 5i 5j", "7e 8e 3j 6e", "7h 8h 7f B0", "6f 6h B1 B2", "8f 8g 6g B3",
+    "4F Q1 Q0 5F", "3F U0 Q3 Q2", "6i 7j 8i 6j", "U1 8j V0 7i", "V1 V2 V3 k00", "k10 V4 k01 k20",
+    "k30 k11 k31 k21", "k40 k41 r10 r20", "r30 r00 r01 r11", "r21 r31 r40 r41", "l0 l1",
 )
 
 

time: 73.3 us -> 75.3 us (1.027)
  Pallas kernels: 72.5 us -> 74.1 us
    pallas_call x1, Pallas kernels: 72.5 us -> 74.1 us  [shards(): pl.pallas_call(kernel, out_shape=jax.ShapeDtypeStruct(stream.shape, strea...]
where the time goes in v8:
time: 75.3 us; the launch traced here: 74.8 us
  Pallas kernels  74.1 us (98%)
    pallas_call x1, Pallas kernels, shards(): pl.pallas_call(kernel, out_shape=jax.ShapeDtypeStruct(stream.shape, strea...  74.1 us

profile of v8, /device:TPU:4, one launch (start us, length us, event | category | flops | bytes accessed | tf_op | source)
XLA Modules:
  0.0 74.8 jit_solution(5812537917538899885)
XLA Ops:
  0.0 74.1 %shard_map.127 = bf16[512,256]{1,0:T(8,128)(2,1)S(1)} custom-call(bf16[512,256]{1,0:T(8,128)(2,1)} %stream_ref.1, f32[1,2048]{1,0:T(1,128)} %bitcast.13, f32[1,2048]{1,0:T(1,128)} %bitcast.14, bf16[2,2,32,256]{3,2,1,0:T(8,128)(2,1)} %bitcast.10, bf16[2,2,32,256]{3,2,1,0:T(8,128)(2,1)} %bitcast.11, bf16[4,256]{1,0:T(4,128)(2,1)} %taps_hbm.1, ...), custom_call_target="tpu_custom_call" | custom-call | tf_op jit(solution)/shard_map/pallas_call | solution.py:650
  74.1 0.7 copy.15
